TPU v7x, 128 devices: a whole 4x4x4 slice. The times are simulated.
128 devices in a mesh: kv: 32 (over z, y, core), tp: 4 (over x).
Axes of the slice: x: 4, y: 4, z: 4, core: 2. Of those that a mesh axis runs over, the one named last changes fastest.
Arguments:
- tokens: bfloat16 [20480, 4096], P('kv'), may hold values from -48 to 48
- query_weight: bfloat16 [4096, 2048], P(None, 'tp'), may hold values from -0.09375 to 0.09375
- key_weight: bfloat16 [4096, 512], P(None, 'tp'), may hold values from -0.09375 to 0.09375
- value_weight: bfloat16 [4096, 512], P(None, 'tp'), may hold values from -0.09375 to 0.09375
- gate_weight: bfloat16 [4096, 64], replicated, may hold values from -0.09375 to 0.09375
- summary_pos: bfloat16 [32, 64], replicated, may hold values from -6 to 6
- key_mixing: bfloat16 [32, 8], replicated, may hold values from -1 to 1
- value_mixing: bfloat16 [32, 8], replicated, may hold values from -1 to 1
- out_weight: bfloat16 [2048, 4096], P('tp'), may hold values from -0.125 to 0.125
- chosen: int32 [320, 8, 16], P('kv', 'tp'), may hold values from 0 to 319, as said below
Outputs:
- mixed: bfloat16 [20480, 4096], P(('kv', 'tp'))
Inputs may be any that keep to these rules, and one draw needn't show every extreme that they name: `chosen`: entry [b, g, 0] is b itself; every entry is at most b. For the query blocks of one index of kv, one key head and any OTHER index of kv, at most 2 distinct blocks of that index's 64-position blocks are named, and exactly 2 of the index just before. Entries may repeat.
All inputs are finite; a program needn't handle non-finite values.
Results may differ from a plain program's by a relative error of at most 0.013.
The roundings to bfloat16 on the way count: a program that leaves them out, or rounds other values in their place, can miss the bound.
Values may be sent and summed in bfloat16 or wider, within the bound.
A program may use at most 192 MiB of HBM per device.

v0:
```python
import jax
import jax.numpy as jnp
from jax import lax
from jax.sharding import Mesh
from jax.sharding import PartitionSpec as P

HD = 64
CMP = 32
SB = 64
N_SEL = 16
KV = ("kv_0", "kv_1", "kv_2")
KV_TP = ("kv_0", "kv_1", "kv_2", "tp")


floor_score = -1e30


def laid_out(pieces, dim):
    shape = list(pieces.shape[1:])
    shape[dim] *= pieces.shape[0]
    return jnp.moveaxis(pieces, 0, dim).reshape(shape)


def all_blocks(x, axes, order):
    pieces = x[None]
    for k in order:
        pieces = lax.all_gather(pieces, axes[k], axis=0, tiled=True)
    held = [lax.axis_size(axes[k]) for k in reversed(order)]
    pieces = pieces.reshape(*held, *x.shape)
    turned = sorted(range(len(order)), key=lambda place: order[len(order) - 1 - place])
    return pieces.transpose(*turned, *range(len(order), pieces.ndim)).reshape(-1, *x.shape)


def gathered_by_axis(x, axes, order, dim):
    return laid_out(all_blocks(x, axes, order), dim)


def masked_weights(scores, visible):
    probs = jax.nn.softmax(jnp.where(visible, scores, floor_score), axis=-1)
    return jnp.where(jnp.any(visible, axis=-1, keepdims=True), probs, 0.0)


def first_named(picked_ids):
    slot_count = picked_ids.shape[-1]
    repeated = picked_ids[..., :, None] == picked_ids[..., None, :]
    earlier = jnp.arange(slot_count)[None, :] < jnp.arange(slot_count)[:, None]
    return jnp.logical_not(jnp.any(repeated & earlier, axis=-1))


def summarize(source, offsets, mixing):
    span_count = source.shape[0] // CMP
    windows = source.astype(jnp.float32).reshape(span_count, CMP, source.shape[1], HD)
    windows = windows + offsets.astype(jnp.float32)[None, :, None, :]
    return jnp.einsum(
        "njgd,jg->ngd", windows, mixing.astype(jnp.float32), precision=lax.Precision.HIGHEST
    ).astype(jnp.bfloat16)


def local(
    tokens,
    query_weight,
    key_weight,
    value_weight,
    gate_weight,
    summary_pos,
    key_mixing,
    value_mixing,
    out_weight,
    chosen,
):
    tok_rows = tokens.shape[0]
    own_index = lax.axis_index(KV)
    head_part = lax.axis_index("tp")
    local_heads = query_weight.shape[1] // HD
    key_heads = key_weight.shape[1] // HD
    group_size = local_heads // key_heads
    own_blocks = tok_rows // SB
    score_scale = HD ** (-0.5)
    queries = jnp.dot(tokens, query_weight, preferred_element_type=jnp.float32).astype(jnp.bfloat16)
    queries = queries.reshape(tok_rows, key_heads, group_size, HD)
    key_rows = jnp.dot(tokens, key_weight, preferred_element_type=jnp.float32).astype(jnp.bfloat16)
    key_rows = key_rows.reshape(tok_rows, key_heads, HD)
    value_rows = jnp.dot(tokens, value_weight, preferred_element_type=jnp.float32).astype(
        jnp.bfloat16
    )
    value_rows = value_rows.reshape(tok_rows, key_heads, HD)
    gate_cols = lax.dynamic_slice_in_dim(
        gate_weight, head_part * local_heads * 2, local_heads * 2, 1
    )
    gate_vals = jax.nn.sigmoid(jnp.dot(tokens, gate_cols, preferred_element_type=jnp.float32))
    gate_vals = gate_vals.reshape(tok_rows, key_heads, group_size, 2)
    key_cols = lax.dynamic_slice_in_dim(key_mixing, head_part * key_heads, key_heads, 1)
    value_cols = lax.dynamic_slice_in_dim(value_mixing, head_part * key_heads, key_heads, 1)
    summary_pair = jnp.concatenate(
        [
            summarize(key_rows, summary_pos, key_cols),
            summarize(value_rows, summary_pos, value_cols),
        ],
        axis=-1,
    )
    summary_all = gathered_by_axis(summary_pair, (("kv_0", "kv_1"), "kv_2"), (0, 1), 0)
    span_ends = jnp.arange(summary_all.shape[0], dtype=jnp.int32) * CMP + (CMP - 1)
    query_pos = own_index * tok_rows + jnp.arange(tok_rows, dtype=jnp.int32)
    summary_scores = (
        jnp.einsum(
            "qgrd,ngd->grqn", queries, summary_all[..., :HD], preferred_element_type=jnp.float32
        )
        * score_scale
    )
    summary_probs = masked_weights(
        summary_scores, (span_ends[None, :] <= query_pos[:, None])[None, None]
    )
    summary_out = jnp.einsum(
        "grqn,ngd->qgrd",
        summary_probs.astype(jnp.bfloat16),
        summary_all[..., HD:],
        preferred_element_type=jnp.float32,
    )
    pair_rows = jnp.concatenate([key_rows, value_rows], axis=-1)
    head_ids = jnp.arange(key_heads, dtype=jnp.int32)[None, :, None]
    whole = lax.all_gather(pair_rows, KV, axis=0, tiled=True)
    block_table = whole.reshape(-1, SB, key_heads, 2 * HD)
    picked = block_table[chosen, :, head_ids, :]
    picked = picked.reshape(own_blocks, key_heads, N_SEL * SB, 2 * HD)
    key_pos = (chosen[..., None] * SB + jnp.arange(SB, dtype=jnp.int32)).reshape(
        own_blocks, key_heads, N_SEL * SB
    )
    unique = first_named(chosen)
    counted = jnp.broadcast_to(unique[..., None], chosen.shape + (SB,)).reshape(
        own_blocks, key_heads, N_SEL * SB
    )
    block_pos = query_pos.reshape(own_blocks, SB)
    visible = counted[:, :, None, None, :] & (
        key_pos[:, :, None, None, :] <= block_pos[:, None, None, :, None]
    )
    query_blocks = queries.reshape(own_blocks, SB, key_heads, group_size, HD)
    chosen_scores = (
        jnp.einsum(
            "bqgrd,bgmd->bgrqm", query_blocks, picked[..., :HD], preferred_element_type=jnp.float32
        )
        * score_scale
    )
    chosen_probs = masked_weights(chosen_scores, visible)
    chosen_out = jnp.einsum(
        "bgrqm,bgmd->bqgrd",
        chosen_probs.astype(jnp.bfloat16),
        picked[..., HD:],
        preferred_element_type=jnp.float32,
    )
    chosen_out = chosen_out.reshape(tok_rows, key_heads, group_size, HD)
    blended = gate_vals[..., 0:1] * summary_out + gate_vals[..., 1:2] * chosen_out
    attention = blended.astype(jnp.bfloat16).reshape(tok_rows, local_heads * HD)
    return lax.psum_scatter(
        jnp.dot(attention, out_weight, preferred_element_type=jnp.float32).astype(jnp.bfloat16),
        "tp",
        scatter_dimension=0,
        tiled=True,
    )


def solution(mesh):
    torus = Mesh(mesh.devices.reshape(4, 4, 2, mesh.shape["tp"]), ("kv_0", "kv_1", "kv_2", "tp"))
    in_specs = (
        P(KV, None),
        P(None, "tp"),
        P(None, "tp"),
        P(None, "tp"),
        P(),
        P(),
        P(),
        P(),
        P("tp", None),
        P(KV, "tp", None),
    )
    out_specs = P(KV_TP, None)
    return jax.shard_map(local, mesh=torus, in_specs=in_specs, out_specs=out_specs, check_vma=False)
```

profile of v0, /device:TPU:1, one launch (start us, length us, event | category | flops | bytes accessed | tf_op | source)
XLA Modules:
  0.0 222.0 jit_solution(7035900383522118441)
XLA Ops:
  6.5 1.2 copy-done
  7.8 4.3 %convolution_convert_fusion.3 = bf16[640,128]{0,1:T(8,128)(2,1)S(1)} fusion(bf16[640,4096]{1,0:T(8,128)(2,1)} %param.10, bf16[4096,128]{1,0:T(8,128)(2,1)S(1)} %copy-done), kind=kOutput, calls=%fused_computation.35 | convolution fusion | flops 671170560 | bytes 6455296 | tf_op jit(solution)/shard_map/dot_general | solution.py:81
  12.1 1.7 convolution_convert_fusion.2
  14.3 0.9 pad_maximum_fusion
  16.7 4.0 %fusion.24 = f32[640,16]{0,1:T(8,128)S(1)} fusion(bf16[640,4096]{1,0:T(8,128)(2,1)} %param.10, bf16[4096,64]{0,1:T(8,128)(2,1)} %param.14, s32[]{:T(128)S(6)} %select_n.27), kind=kOutput, calls=%fused_computation.40 | convolution fusion | flops 83916800 | bytes 5414916 | tf_op jit(solution)/shard_map/dot_general | solution.py:90
  23.8 22.3 %all-gather = bf16[320,2,128]{2,1,0:T(2,128)(2,1)S(1)} all-gather(bf16[20,2,128]{2,1,0:T(2,128)(2,1)S(1)} %pad_maximum_fusion.1), channel_id=2, replica_groups=mesh['kv_0'=4,'kv_1'=4,'kv_2'=2,'tp'=4] {'kv_0','kv_1'}, dimensions={0}, use_global_device_ids=true | all-gather | bytes 174080 | tf_op jit(solution)/shard_map/all_gather | solution.py:27
  46.2 6.5 %all_gather.10 = bf16[32,20,2,128]{3,2,1,0:T(2,128)(2,1)S(1)} all-gather(bf16[16,20,2,128]{3,2,1,0:T(2,128)(2,1)S(1)} %bitcast.142), channel_id=1, replica_groups=mesh['kv_0'=4,'kv_1'=4,'kv_2'=2,'tp'=4] {'kv_2'}, dimensions={0}, use_global_device_ids=true | all-gather | bytes 491520 | tf_op jit(solution)/shard_map/all_gather | solution.py:27
  53.6 0.8 copy.85
  54.6 7.6 %convolution_convert_fusion.1 = bf16[640,512]{0,1:T(8,128)(2,1)S(1)} fusion(bf16[640,4096]{1,0:T(8,128)(2,1)} %param.10, bf16[4096,512]{1,0:T(8,128)(2,1)} %param.11), kind=kOutput, calls=%fused_computation.31 | convolution fusion | flops 2684682240 | bytes 10092544 | tf_op jit(solution)/shard_map/dot_general | solution.py:79
  62.2 1.2 reshape.189
  64.3 1.6 and_reduce_fusion
  66.2 2.2 %compare_and_fusion = pred[10,2,64,1024]{3,2,1,0:T(8,128)(4,1)} fusion(s32[10,64]{1,0:T(8,128)S(1)} %add_add_fusion, s32[10,2,1024]{2,1,0:T(2,128)S(1)} %broadcast_add_fusion.2, pred[10,2,1024]{2,1,0:T(4,128)(4,1)S(1)} %copy.63), kind=kLoop, calls=%fused_computation.23 | loop fusion | flops 2621440 | bytes 1415680 | tf_op jit(solution)/shard_map/and | solution.py:133
  68.5 7.4 %fusion.57 = (f32[2,4,640]{2,1,0:T(4,128)S(1)}, f32[2,4,640,640]{2,3,1,0:T(8,128)}) fusion(pred[640,640]{0,1:T(8,128)(4,1)S(1)} %broadcast_compare_fusion, bf16[640,2,4,64]{0,3,2,1:T(8,128)(2,1)S(1)} %bitcast.143, bf16[640,2,64]{0,2,1:T(8,128)(2,1)S(1)} %copy.86), kind=kOutput, calls=%fused_computation.88 | convolution fusion | flops 432538240 | bytes 14356480 | tf_op jit(solution)/shard_map/sub | solution.py:39
  75.9 1.0 all-gather.3.cloned.1.call-done
  76.9 11.6 %copy.60 = bf16[320,64,2,128]{3,1,2,0:T(8,128)(2,1)} copy(bf16[320,64,2,128]{3,1,0,2:T(8,128)(2,1)} %bitcast.135) | data formatting | bytes 20971520 | tf_op jit(solution)/shard_map/reshape | solution.py:122
  88.5 9.0 %gather_fusion = bf16[320,64,128]{2,1,0:T(8,128)(2,1)} fusion(bf16[320,64,2,128]{3,1,2,0:T(8,128)(2,1)} %copy.60, s32[320]{0:T(512)S(1)} %reshape.168), kind=kCustom, calls=%fused_computation | custom fusion | bytes 10488320 | tf_op jit(solution)/shard_map/gather | solution.py:123
  97.5 11.1 %fusion.12 = f32[10,2,1024,64,4]{2,3,4,1,0:T(8,128)} fusion(bf16[10,2,1024,128]{3,2,1,0:T(8,128)(2,1)} %bitcast.131, bf16[10,64,2,4,64]{1,0,4,3,2:T(8,128)(2,1)S(1)} %reshape.189), kind=kOutput, calls=%fused_computation.21 | convolution fusion | flops 671088640 | bytes 26869760 | tf_op jit(solution)/shard_map/bqgrd,bgmd->bgrqm/dot_general | solution.py:138
  108.7 22.2 %fusion.62 = (f32[10,2,4,64]{3,2,1,0:T(4,128)S(1)}, f32[10,2,4,64,1024]{4,3,2,1,0:T(8,128)}) fusion(f32[10,2,1024,64,4]{2,3,4,1,0:T(8,128)} %fusion.12, pred[10,2,64,1024]{3,2,1,0:T(8,128)(4,1)} %compare_and_fusion), kind=kOutput, calls=%fused_computation.89 | output fusion | flops 31458304 | bytes 43274240 | tf_op jit(solution)/shard_map/sub | solution.py:39
  131.0 13.0 %fusion.13 = f32[10,64,2,4,64]{1,4,3,2,0:T(8,128)} fusion(f32[10,2,4,64,1024]{4,3,2,1,0:T(8,128)} %get-tuple-element.14, f32[10,2,4,64]{3,2,1,0:T(4,128)S(1)} %get-tuple-element.13, pred[10,2,64]{2,1,0:T(4,128)(4,1)S(1)} %copy-done.8, bf16[10,2,1024,128]{3,2,1,0:T(8,128)(2,1)S(1)} %bitcast.134), kind=kOutput, calls=%fused_computation.25 | convolution fusion | flops 686817280 | bytes 27546880 | tf_op jit(solution)/shard_map/bgrqm,bgmd->bqgrd/dot_general | solution.py:144
  143.9 3.3 %copy.68 = f32[10,64,2,4,64]{4,1,0,3,2:T(8,128)} copy(f32[10,64,2,4,64]{1,4,3,2,0:T(8,128)} %fusion.13) | data formatting | bytes 2621440 | tf_op jit(solution)/shard_map/bgrqm,bgmd->bqgrd/transpose | solution.py:144
  147.3 2.1 copy.69
  149.4 6.5 %fusion.19 = bf16[640,2,4,64]{0,3,2,1:T(8,128)(2,1)S(1)} fusion(f32[2,4,640,640]{2,3,1,0:T(8,128)} %get-tuple-element.12, f32[2,4,640]{2,1,0:T(4,128)S(1)} %get-tuple-element.11, pred[640]{0:T(1024)(128)(4,1)S(1)} %copy-done.9, f32[640,2,4,64]{0,3,2,1:T(8,128)S(1)} %copy.69, f32[640,2,4]{0,2,1:T(4,128)S(1)} %get-tuple-element.19, ...), kind=kOutput, calls=%fused_computation.32 | convolution fusion | flops 430571520 | bytes 15299200 | tf_op jit(solution)/shard_map/grqn,ngd->qgrd/dot_general | solution.py:113
  155.9 4.7 %convolution_convert_fusion = bf16[640,4096]{1,0:T(8,128)(2,1)} fusion(bf16[640,512]{0,1:T(8,128)(2,1)S(1)} %bitcast.141, bf16[512,4096]{1,0:T(8,128)(2,1)S(1)} %copy-done.3), kind=kOutput, calls=%fused_computation.19 | convolution fusion | flops 2686976000 | bytes 10092544 | tf_op jit(solution)/shard_map/dot_general | solution.py:154
  160.7 54.5 %reduce-scatter.2.cloned.1.call-done = bf16[160,4096]{1,0:T(8,128)(2,1)} async-done(((bf16[640,4096]{1,0:T(8,128)(2,1)}), bf16[160,4096]{1,0:T(8,128)(2,1)}) %reduce-scatter.2.cloned.1.call-update) | async-done | bytes 1310736 | tf_op jit(solution)/shard_map/reduce_scatter | solution.py:153
  (68 shorter events, 7.2 us)
Async XLA Ops:
  6.5 1.2 copy-start
  6.5 5.5 %copy-start.4 = (bf16[4096,128]{1,0:T(8,128)(2,1)S(1)}, bf16[4096,128]{1,0:T(8,128)(2,1)}, u32[]{:S(2)}) copy-start(bf16[4096,128]{1,0:T(8,128)(2,1)} %param.13) | copy-start | bytes 3145732
  6.5 70.3 %all-gather.3.cloned.1.call-start = ((), (), s32[]{:S(2)}) async-start(), calls=%async_computation.1 | async-start | bytes 10813440 | tf_op jit(solution)/shard_map/all_gather | solution.py:121
  7.8 4.3 %copy-start.2 = (bf16[640,4096]{1,0:T(8,128)(2,1)S(1)}, bf16[640,4096]{1,0:T(8,128)(2,1)}, u32[]{:S(2)}) copy-start(bf16[640,4096]{1,0:T(8,128)(2,1)} %param.10) | copy-start | bytes 15728644
  12.1 3.5 %copy-start.5 = (s32[10,2,16]{2,1,0:T(2,128)S(1)}, s32[10,2,16]{2,1,0:T(2,128)}, u32[]{:S(2)}) copy-start(s32[10,2,16]{2,1,0:T(2,128)} %param.19) | copy-start | bytes 3844
  12.1 4.3 %copy-start.7 = (bf16[32,64]{1,0:T(8,128)(2,1)S(1)}, bf16[32,64]{1,0:T(8,128)(2,1)}, u32[]{:S(2)}) copy-start(bf16[32,64]{1,0:T(8,128)(2,1)} %param.15) | copy-start | bytes 12292
  15.3 199.9 %reduce-scatter.2.cloned.1.call-start = ((), (), s32[]{:S(2)}) async-start(), calls=%async_computation.2 | async-start | bytes 6553600 | tf_op jit(solution)/shard_map/reduce_scatter | solution.py:153
  97.5 33.4 %slice-start = ((s8[5242880]{0:T(1024)(128)(4,1)}), s8[4194304]{0:T(1024)(128)(4,1)S(1)}, s32[]{:S(2)}) async-start(s8[5242880]{0:T(1024)(128)(4,1)} %bitcast.132), calls=%async_computation.3 | async-start | bytes 8388608
  108.7 22.3 %slice-start.1 = ((s8[5242880]{0:T(1024)(128)(4,1)}), s8[1048576]{0:T(1024)(128)(4,1)S(1)}, s32[]{:S(2)}) async-start(s8[5242880]{0:T(1024)(128)(4,1)} %bitcast.132), calls=%async_computation.4 | async-start | bytes 2097152
  108.7 22.3 %copy-start.8 = (pred[10,2,64]{2,1,0:T(4,128)(4,1)S(1)}, pred[10,2,64]{2,1,0:T(4,128)(4,1)}, u32[]{:S(2)}) copy-start(pred[10,2,64]{2,1,0:T(4,128)(4,1)} %and_reduce_fusion) | copy-start | bytes 3844
  143.9 5.5 %copy-start.6 = (bf16[640,2,64]{0,2,1:T(8,128)(2,1)S(1)}, bf16[640,2,64]{0,2,1:T(8,128)(2,1)}, u32[]{:S(2)}) copy-start(bf16[640,2,64]{0,2,1:T(8,128)(2,1)} %copy.85) | copy-start | bytes 491524
  143.9 5.5 %copy-start.9 = (pred[640]{0:T(1024)(128)(4,1)S(1)}, pred[640]{0:T(1024)(128)(4,1)}, u32[]{:S(2)}) copy-start(pred[640]{0:T(1024)(128)(4,1)} %compare_reduce_fusion) | copy-start | bytes 1924
  149.4 6.5 %copy-start.3 = (bf16[512,4096]{1,0:T(8,128)(2,1)S(1)}, bf16[512,4096]{1,0:T(8,128)(2,1)}, u32[]{:S(2)}) copy-start(bf16[512,4096]{1,0:T(8,128)(2,1)} %param.18) | copy-start | bytes 12582916
  155.9 59.3 %copy-start.1 = (bf16[4096,128]{1,0:T(8,128)(2,1)S(1)}, bf16[4096,128]{1,0:T(8,128)(2,1)}, u32[]{:S(2)}) copy-start(bf16[4096,128]{1,0:T(8,128)(2,1)} %param.12) | copy-start | bytes 3145732
Sparse Core Ops, SparseCore 0:
  15.4 61.4 all-gather.2
  160.8 54.3 reduce-scatter.1
where the time goes:
time: 222 us
  matrix products  61.1 us (28%)
  waiting for transfers between devices  55.5 us (25%)
  local copies, waits for them, and re-layouts  33.5 us (15%)
  other arithmetic  29.3 us (13%)
  blocking collectives  28.8 us (13%)
  between operations  13.8 us (6%)
    reduce_scatter x1, waiting for transfers between devices, local(): lax.psum_scatter(jnp.dot(attention, out_weight, preferred_element_type=jn...  54.5 us
    all_gather x2, blocking collectives, all_blocks(): pieces = lax.all_gather(pieces, axes[k], axis=0, tiled=True)  28.8 us
    sub x1, other arithmetic, masked_weights(): probs = jax.nn.softmax(jnp.where(visible, scores, floor_score), axis=-1)  22.2 us
    dot_general x1, matrix products, local(): jnp.einsum('bgrqm,bgmd->bqgrd', chosen_probs.astype(jnp.bfloat16), picked...  13 us
    reshape x1, local copies, waits for them, and re-layouts, local(): block_table = whole.reshape(-1, SB, key_heads, 2 * HD)  11.6 us
    dot_general x1, matrix products, local(): jnp.einsum('bqgrd,bgmd->bgrqm', query_blocks, picked[..., :HD], preferred...  11.1 us
    gather x1, local copies, waits for them, and re-layouts, local(): picked = block_table[chosen, :, head_ids, :]  9.01 us
    dot_general x1, matrix products, local(): jnp.dot(tokens, query_weight, preferred_element_type=jnp.float32)  7.6 us
  transfers between devices with their start and end apart: 2, of which 2 were waited for; matrix products, arithmetic and copies ran while one was open for 14% of the time, Pallas kernels for 0%

commit v1 on v0

v1 whole, which is shorter than its diff:
```python
import jax
import jax.numpy as jnp
from jax import lax
from jax.experimental import pallas as pl
from jax.experimental.pallas import tpu as pltpu
from jax.sharding import Mesh
from jax.sharding import PartitionSpec as P

HD = 64
CMP = 32
SB = 64
N_SEL = 16
N_KV = 32
N_TP = 4
ROWS = 640
BLOCKS = 10
GROUPS = 2
GROUP = 4
SPANS = 20
WIDTH = 512
D = 4096
CHUNK = 1024
KV = ("kv_0", "kv_1", "kv_2")
KV_TP = ("kv_0", "kv_1", "kv_2", "tp")
MESH = pl.DeviceIdType.MESH
BF16 = jnp.bfloat16
F32 = jnp.float32
LOW = -1e30


def nt_dot(a, b):
    return lax.dot_general(a, b, (((1,), (1,)), ((), ())), preferred_element_type=F32)


def nn_dot(a, b):
    return jnp.dot(a, b, preferred_element_type=F32)


def body(
    tok_hbm,
    wq_hbm,
    wk_hbm,
    wv_hbm,
    wg_hbm,
    pos_ref,
    kmix_ref,
    vmix_ref,
    need_ref,
    idx_ref,
    bias_ref,
    out_ref,
    tok,
    wq,
    wkv,
    wg,
    acc,
    gates,
    qp,
    sums,
    asked,
    asked_s,
    table,
    stage,
    mine,
    comp,
    load_sem,
    asked_sem,
    need_send,
    need_recv,
    sum_send,
    sum_recv,
    blk_send,
    blk_recv,
):
    kz, ky, kc, x = (lax.axis_index(name) for name in KV_TP)
    me = kz * 8 + ky * 2 + kc

    def at(d):
        return (d // 8, lax.rem(d // 2, 4), lax.rem(d, 2), x)

    barrier = pltpu.get_barrier_semaphore()

    def greet(d, carry):
        @pl.when(d != me)
        def _():
            pl.semaphore_signal(barrier, inc=1, device_id=at(d), device_id_type=MESH)

        return carry

    lax.fori_loop(0, N_KV, greet, 0)

    loads = []

    def load(src, dst):
        loads.append(pltpu.make_async_copy(src, dst, load_sem.at[len(loads)]))
        loads[-1].start()
        return loads[-1]

    steps = D // CHUNK
    kv_loads = []
    for k in range(steps):
        rows = pl.ds(k * CHUNK, CHUNK)
        kv_loads.append(
            (
                load(wk_hbm.at[rows], wkv.at[rows, pl.ds(0, 128)]),
                load(wv_hbm.at[rows], wkv.at[rows, pl.ds(128, 128)]),
                load(tok_hbm.at[:, rows], tok.at[:, rows]),
            )
        )
    wg_load = load(wg_hbm, wg)
    wq_load = load(wq_hbm, wq)

    def clear(d, carry):
        sums[d] = jnp.zeros(sums.shape[1:], BF16)
        return carry

    lax.fori_loop(me + 1, N_KV, clear, 0)
    pl.semaphore_wait(barrier, N_KV - 1)

    def need_copy(d, sender):
        return pltpu.make_async_remote_copy(
            src_ref=need_ref.at[d],
            dst_ref=asked.at[sender],
            send_sem=need_send.at[d],
            recv_sem=need_recv.at[sender],
            device_id=at(d),
            device_id_type=MESH,
        )

    def send_need(d, carry):
        need_copy(d, me).start()
        return carry

    lax.fori_loop(0, me, send_need, 0)

    for k in range(steps):
        for copy in kv_loads[k]:
            copy.wait()
        part = nn_dot(tok[:, k * CHUNK : (k + 1) * CHUNK], wkv[k * CHUNK : (k + 1) * CHUNK])
        acc[...] = part if k == 0 else acc[...] + part
    low = lax.broadcasted_iota(jnp.int32, (ROWS, 128), 1) < HD
    keys = acc[:, :128].astype(BF16).astype(F32)
    values = acc[:, 128:].astype(BF16).astype(F32)
    pairs = (
        jnp.where(low, keys, pltpu.roll(values, HD, 1)),
        jnp.where(low, pltpu.roll(keys, HD, 1), values),
    )
    offsets = pos_ref[...].astype(F32)
    offsets = jnp.concatenate([offsets, offsets], axis=1)
    lane_low = lax.broadcasted_iota(jnp.int32, (CMP, 128), 1) < HD
    lane_head = lax.broadcasted_iota(jnp.int32, (CMP, 8), 1)
    for g in range(GROUPS):
        pair = pairs[g]
        blocks = pair.astype(BF16).reshape(BLOCKS, SB, 128)
        mine[g] = blocks
        table[4 * N_KV + g * BLOCKS : 4 * N_KV + (g + 1) * BLOCKS] = blocks
        own = lane_head == x * GROUPS + g
        kmix = jnp.sum(jnp.where(own, kmix_ref[...].astype(F32), 0.0), axis=1, keepdims=True)
        vmix = jnp.sum(jnp.where(own, vmix_ref[...].astype(F32), 0.0), axis=1, keepdims=True)
        mixing = jnp.where(lane_low, kmix, vmix)
        spans = jnp.sum((pair.reshape(SPANS, CMP, 128) + offsets[None]) * mixing[None], axis=1)
        sums[me, 0, g] = spans[:16].astype(BF16)
        sums[me, 1, g] = jnp.concatenate([spans[16:], jnp.zeros((12, 128), F32)], axis=0).astype(
            BF16
        )

    def sum_copy(d, sender):
        return pltpu.make_async_remote_copy(
            src_ref=sums.at[sender],
            dst_ref=sums.at[sender],
            send_sem=sum_send.at[d],
            recv_sem=sum_recv.at[sender],
            device_id=at(d),
            device_id_type=MESH,
        )

    def send_sum(d, carry):
        sum_copy(d, me).start()
        return carry

    lax.fori_loop(me + 1, N_KV, send_sum, 0)

    def take_need(d, carry):
        need_copy(me, d).wait_recv()
        copy = pltpu.make_async_copy(asked.at[d], asked_s.at[d], asked_sem.at[d])
        copy.start()
        return carry

    lax.fori_loop(me + 1, N_KV, take_need, 0)

    def blk_copy(d, sender):
        return pltpu.make_async_remote_copy(
            src_ref=stage.at[d],
            dst_ref=table.at[pl.ds(sender * 4, 4)],
            send_sem=blk_send.at[d],
            recv_sem=blk_recv.at[sender],
            device_id=at(d),
            device_id_type=MESH,
        )

    def send_blk(d, carry):
        pltpu.make_async_copy(asked.at[d], asked_s.at[d], asked_sem.at[d]).wait()
        for slot in range(4):
            block = asked_s[d, 0, slot]
            stage[d, slot] = mine[slot // 2, block]
        blk_copy(d, me).start()
        return carry

    lax.fori_loop(me + 1, N_KV, send_blk, 0)

    wq_load.wait()
    for g in range(GROUPS):
        cols = slice(256 * g, 256 * (g + 1))
        for k in range(steps):
            ks = slice(k * CHUNK, (k + 1) * CHUNK)
            part = nn_dot(tok[:, ks], wq[ks, cols])
            acc[...] = part if k == 0 else acc[...] + part
        for r in range(GROUP):
            tile = acc[:, 128 * (r // 2) : 128 * (r // 2) + 128]
            if r % 2:
                tile = pltpu.roll(tile, HD, 1)
            tile = jnp.where(low, tile, 0.0).astype(BF16) * BF16(HD**-0.5)
            qp[:, g, r] = tile.reshape(BLOCKS, SB, 128)
    wg_load.wait()
    pick = lax.broadcasted_iota(jnp.int32, (64, 128), 0) == (
        lax.broadcasted_iota(jnp.int32, (64, 128), 1) + x * 16
    )
    own_gates = nn_dot(wg[...], jnp.where(pick, 1.0, 0.0).astype(BF16)).astype(BF16)
    gates[...] = jax.nn.sigmoid(nn_dot(tok[...], own_gates)).reshape(BLOCKS, SB, 128)

    def take_sum(s, carry):
        sum_copy(me, s).wait_recv()
        return carry

    lax.fori_loop(0, me, take_sum, 0)
    lane_a = lax.broadcasted_iota(jnp.int32, (GROUP * SB, 512), 1)
    end_a = ((lane_a // 16) * SPANS + lax.rem(lane_a, 16)) * CMP + CMP - 1
    lane_b = lax.broadcasted_iota(jnp.int32, (GROUP * SB, 128), 1)
    end_b = ((lane_b // 4) * SPANS + 16 + lax.rem(lane_b, 4)) * CMP + CMP - 1
    row_a = lax.rem(lax.broadcasted_iota(jnp.int32, (GROUP * SB, 512), 0), SB)
    row_b = lax.rem(lax.broadcasted_iota(jnp.int32, (GROUP * SB, 128), 0), SB)
    row_c = lax.rem(lax.broadcasted_iota(jnp.int32, (GROUP * SB, 1), 0), SB)
    gap_a = end_a - row_a
    gap_b = end_b - row_b

    def gate_cols(b, g, branch):
        cols = [
            gates[b][:, 2 * (GROUP * g + r) + branch : 2 * (GROUP * g + r) + branch + 1]
            for r in range(GROUP)
        ]
        return jnp.concatenate(cols, axis=0)

    for g in range(GROUPS):
        span_a = sums[:, 0, g].reshape(N_KV * 16, 128)
        span_b = jnp.concatenate([sums[s, 1, g].astype(F32)[:4] for s in range(N_KV)], axis=0)
        span_b = span_b.astype(BF16)

        def compressed(b, carry):
            q = qp[b, g].reshape(GROUP * SB, 128)
            start = me * ROWS + b * SB
            score_a = jnp.where(gap_a <= start, nt_dot(q, span_a), LOW)
            score_b = jnp.where(gap_b <= start, nt_dot(q, span_b), LOW)
            most = jnp.maximum(
                jnp.max(score_a, axis=1, keepdims=True), jnp.max(score_b, axis=1, keepdims=True)
            )
            prob_a = jnp.exp(score_a - most)
            prob_b = jnp.exp(score_b - most)
            total = jnp.sum(prob_a, axis=1, keepdims=True) + jnp.sum(prob_b, axis=1, keepdims=True)
            mixed = nn_dot(prob_a.astype(BF16), span_a) + nn_dot(prob_b.astype(BF16), span_b)
            sees = row_c + start >= CMP - 1
            factor = jnp.where(sees, gate_cols(b, g, 0) / total, 0.0)
            comp[b, g] = mixed * factor
            return carry

        lax.fori_loop(0, BLOCKS, compressed, 0)

    def take_blk(s, carry):
        blk_copy(me, s).wait_recv()
        return carry

    lax.fori_loop(0, me, take_blk, 0)
    lane_first = lax.broadcasted_iota(jnp.int32, (GROUP * SB, 128), 1)
    causal = jnp.logical_or(lane_first >= SB, lane_first <= row_b)
    low_half = lax.broadcasted_iota(jnp.int32, (SB, 128), 1) < HD

    def chosen_block(b, carry):
        for g in range(GROUPS):
            q = qp[b, g].reshape(GROUP * SB, 128)
            base = (b * GROUPS + g) * N_SEL
            picked = jnp.concatenate([table[idx_ref[base + s]] for s in range(N_SEL)], axis=0)
            score = nt_dot(q, picked) + bias_ref[b * GROUPS + g]
            head = jnp.where(causal, score[:, :128], LOW)
            score = jnp.concatenate([head, score[:, 128:]], axis=1)
            most = jnp.max(score, axis=1, keepdims=True)
            prob = jnp.exp(score - most)
            total = jnp.sum(prob, axis=1, keepdims=True)
            mixed = nn_dot(prob.astype(BF16), picked)
            both = comp[b, g] + mixed * (gate_cols(b, g, 1) / total)
            for half in range(2):
                even = both[(2 * half) * SB : (2 * half + 1) * SB]
                odd = both[(2 * half + 1) * SB : (2 * half + 2) * SB]
                tile = jnp.where(low_half, pltpu.roll(even, HD, 1), odd).astype(BF16)
                lanes = slice(256 * g + 128 * half, 256 * g + 128 * half + 128)
                out_ref[pl.ds(pl.multiple_of(b * SB, SB), SB), lanes] = tile
        return carry

    lax.fori_loop(0, BLOCKS, chosen_block, 0)

    def sent_need(d, carry):
        need_copy(d, me).wait_send()
        return carry

    lax.fori_loop(0, me, sent_need, 0)

    def sent_rest(d, carry):
        sum_copy(d, me).wait_send()
        blk_copy(d, me).wait_send()
        return carry

    lax.fori_loop(me + 1, N_KV, sent_rest, 0)


def plan(chosen, me):
    named = chosen.transpose(1, 0, 2).reshape(GROUPS, BLOCKS * N_SEL)
    source = named // BLOCKS
    place = named - source * BLOCKS
    hit = source[:, None, :] == jnp.arange(N_KV, dtype=jnp.int32)[None, :, None]
    first = jnp.min(jnp.where(hit, place[:, None, :], BLOCKS), axis=2)
    last = jnp.max(jnp.where(hit, place[:, None, :], 0), axis=2)
    first_there = jnp.sum(jnp.where(hit, first[:, :, None], 0), axis=1)
    first = jnp.where(first == BLOCKS, 0, first)
    group = jnp.arange(GROUPS, dtype=jnp.int32)[:, None]
    far = (source * GROUPS + group) * 2 + (place != first_there).astype(jnp.int32)
    near = 4 * N_KV + group * BLOCKS + place
    index = jnp.where(source == me, near, far)
    index = index.reshape(GROUPS, BLOCKS, N_SEL).transpose(1, 0, 2).reshape(-1)
    need = jnp.stack([first, last], axis=-1).transpose(1, 0, 2).reshape(N_KV, 1, 2 * GROUPS)
    need = jnp.pad(need, ((0, 0), (0, 0), (0, 128 - 2 * GROUPS)))
    same = chosen[..., :, None] == chosen[..., None, :]
    slot = jnp.arange(N_SEL, dtype=jnp.int32)
    repeated = jnp.any(same & (slot[None, :] < slot[:, None]), axis=-1)
    bias = jnp.where(repeated, LOW, 0.0).astype(F32)
    bias = jnp.repeat(bias, SB, axis=-1).reshape(BLOCKS * GROUPS, 1, N_SEL * SB)
    return need, index, bias


def local(
    tokens,
    query_weight,
    key_weight,
    value_weight,
    gate_weight,
    summary_pos,
    key_mixing,
    value_mixing,
    out_weight,
    chosen,
):
    need, index, bias = plan(chosen, lax.axis_index(KV))
    any_space = pl.BlockSpec(memory_space=pl.ANY)
    vmem = pl.BlockSpec(memory_space=pltpu.VMEM)
    smem = pl.BlockSpec(memory_space=pltpu.SMEM)
    dma = pltpu.SemaphoreType.DMA
    attention = pl.pallas_call(
        body,
        out_shape=jax.ShapeDtypeStruct((ROWS, WIDTH), BF16),
        in_specs=[any_space] * 5 + [vmem] * 4 + [smem, vmem],
        out_specs=vmem,
        scratch_shapes=[
            pltpu.VMEM((ROWS, D), BF16),
            pltpu.VMEM((D, WIDTH), BF16),
            pltpu.VMEM((D, 256), BF16),
            pltpu.VMEM((D, 64), BF16),
            pltpu.VMEM((ROWS, 256), F32),
            pltpu.VMEM((BLOCKS, SB, 128), F32),
            pltpu.VMEM((BLOCKS, GROUPS, GROUP, SB, 128), BF16),
            pltpu.VMEM((N_KV, 2, GROUPS, 16, 128), BF16),
            pltpu.VMEM((N_KV, 1, 128), jnp.int32),
            pltpu.SMEM((N_KV, 1, 128), jnp.int32),
            pltpu.VMEM((4 * N_KV + GROUPS * BLOCKS, SB, 128), BF16),
            pltpu.VMEM((N_KV, 4, SB, 128), BF16),
            pltpu.VMEM((GROUPS, BLOCKS, SB, 128), BF16),
            pltpu.VMEM((BLOCKS, GROUPS, GROUP * SB, 128), F32),
            dma((16,)),
            dma((N_KV,)),
            dma((N_KV,)),
            dma((N_KV,)),
            dma((N_KV,)),
            dma((N_KV,)),
            dma((N_KV,)),
            dma((N_KV,)),
        ],
        compiler_params=pltpu.CompilerParams(
            collective_id=0, has_side_effects=True, vmem_limit_bytes=63 * 1024 * 1024
        ),
    )(
        tokens,
        query_weight,
        key_weight,
        value_weight,
        gate_weight,
        summary_pos,
        key_mixing,
        value_mixing,
        need,
        index,
        bias,
    )
    return lax.psum_scatter(
        jnp.dot(attention, out_weight, preferred_element_type=F32).astype(BF16),
        "tp",
        scatter_dimension=0,
        tiled=True,
    )


def solution(mesh):
    torus = Mesh(mesh.devices.reshape(4, 4, 2, mesh.shape["tp"]), ("kv_0", "kv_1", "kv_2", "tp"))
    in_specs = (
        P(KV, None),
        P(None, "tp"),
        P(None, "tp"),
        P(None, "tp"),
        P(),
        P(),
        P(),
        P(),
        P("tp", None),
        P(KV, "tp", None),
    )
    out_specs = P(KV_TP, None)
    return jax.shard_map(local, mesh=torus, in_specs=in_specs, out_specs=out_specs, check_vma=False)
```

time: 222 us -> 152 us (0.68)
  matrix products: 61.1 us -> 7.59 us
  Pallas kernels: 0 us -> 50 us
  blocking collectives: 28.8 us -> 0 us
  other arithmetic: 29.3 us -> 2.36 us
  local copies, waits for them, and re-layouts: 33.5 us -> 8.19 us
  waiting for transfers between devices: 55.5 us -> 69.8 us
    pallas_call x0 -> x1, Pallas kernels: none -> 50 us  [local(): pl.pallas_call(body, out_shape=jax.ShapeDtypeStruct((ROWS, WIDTH), BF16),...]
    dot_general x10 -> x1, matrix products: 53.7 us -> 7.59 us  [local(): jnp.dot(attention, out_weight, preferred_element_type=F32).astype(BF16)]
    all_gather x2 -> x0, blocking collectives: 28.8 us -> none  [all_blocks(): pieces = lax.all_gather(pieces, axes[k], axis=0, tiled=True)]
    sub x1, other arithmetic: 22.2 us -> 0.02 us  [plan(): place = named - source * BLOCKS]
    reduce_scatter x1, waiting for transfers between devices: 54.5 us -> 69.8 us  [local(): lax.psum_scatter(jnp.dot(attention, out_weight, preferred_element_type=F3...]
    reshape x5 -> x3, local copies, waits for them, and re-layouts: 14.2 us -> 0.85 us  [the longest x1 0.68 us: plan(): index = index.reshape(GROUPS, BLOCKS, N_SEL).transpose(1, 0, 2).reshape(-1)]
    gather x1 -> x0, local copies, waits for them, and re-layouts: 9.01 us -> none  [local(): picked = block_table[chosen, :, head_ids, :]]
    sub x1 -> x0, matrix products: 7.41 us -> none  [masked_weights(): probs = jax.nn.softmax(jnp.where(visible, scores, floor_score), axis=-1)]
  transfers between devices with their start and end apart: 2 -> 1, of which waited for: 2 -> 1; matrix products, arithmetic and copies ran while one was open for 14% -> 0% of each run, Pallas kernels for 0% -> 0%
where the time goes in v1:
time: 152 us; the launch traced here: 151 us
  waiting for transfers between devices  69.8 us (46%)
  Pallas kernels  50 us (33%)
  between operations  13.4 us (9%)
  local copies, waits for them, and re-layouts  8.19 us (5%)
  matrix products  7.59 us (5%)
  other arithmetic  2.36 us (2%)
    reduce_scatter x1, waiting for transfers between devices, local(): lax.psum_scatter(jnp.dot(attention, out_weight, preferred_element_type=F3...  69.8 us
    pallas_call x1, Pallas kernels, local(): pl.pallas_call(body, out_shape=jax.ShapeDtypeStruct((ROWS, WIDTH), BF16),...  50 us
    dot_general x1, matrix products, local(): jnp.dot(attention, out_weight, preferred_element_type=F32).astype(BF16)  7.59 us
    unnamed x4, local copies, waits for them, and re-layouts  5.77 us
  transfers between devices with their start and end apart: 1, of which 1 were waited for; matrix products, arithmetic and copies ran while one was open for 0% of the time, Pallas kernels for 0%

profile of v1, /device:TPU:1, one launch (start us, length us, event | category | flops | bytes accessed | tf_op | source)
XLA Modules:
  0.0 151.4 jit_solution(10227946323427896341)
XLA Ops:
  6.5 0.0 reduce-scatter.2.cloned.1.call-start
  6.5 0.7 copy.39
  7.3 0.1 reshape.81
  7.4 0.2 select_reduce_fusion.2
  7.5 0.1 select_reduce_fusion
  7.6 1.3 and_reduce_fusion
  8.9 1.4 copy.34.kmix_ref
  10.3 1.4 copy.35.vmix_ref
  11.7 0.1 copy.31
  11.8 0.1 reduce_sum.12
  11.8 0.8 select_bitcast_fusion
  12.6 0.7 reshape.83.idx_ref
  13.3 0.1 broadcast_in_dim.61
  13.4 0.8 reshape_reshape.3.bias_ref
  14.2 2.4 %copy.33.wg_hbm = bf16[4096,64]{1,0:T(8,128)(2,1)} copy(bf16[4096,64]{0,1:T(8,128)(2,1)} %param.14) | data formatting | bytes 1048576 | tf_op args[4]
  16.5 0.6 pad.4.need_ref
  17.1 50.0 %shard_map.100 = bf16[640,512]{1,0:T(8,128)(2,1)} custom-call(bf16[640,4096]{1,0:T(8,128)(2,1)} %tok_hbm.1, bf16[4096,512]{1,0:T(8,128)(2,1)} %wq_hbm.1, bf16[4096,128]{1,0:T(8,128)(2,1)} %wk_hbm.1, bf16[4096,128]{1,0:T(8,128)(2,1)} %wv_hbm.1, bf16[4096,64]{1,0:T(8,128)(2,1)} %copy.33.wg_hbm, bf16[32,64]{1,0:T(8,128)(2,1)} %pos_ref.1, ...), custom_call_target="tpu_custom_call" | custom-call | tf_op jit(solution)/shard_map/pallas_call | solution.py:364
  67.1 7.6 %convolution_convert_fusion = bf16[640,4096]{1,0:T(8,128)(2,1)} fusion(bf16[640,512]{1,0:T(8,128)(2,1)} %shard_map.100, bf16[512,4096]{1,0:T(8,128)(2,1)} %param.18), kind=kOutput, calls=%fused_computation | convolution fusion | flops 2686976000 | bytes 10092544 | tf_op jit(solution)/shard_map/dot_general | solution.py:410
  74.7 0.0 reduce-scatter.2.cloned.1.call-update
  74.7 69.8 %reduce-scatter.2.cloned.1.call-done = bf16[160,4096]{1,0:T(8,128)(2,1)} async-done(((bf16[640,4096]{1,0:T(8,128)(2,1)}), bf16[160,4096]{1,0:T(8,128)(2,1)}) %reduce-scatter.2.cloned.1.call-update) | async-done | bytes 1310736 | tf_op jit(solution)/shard_map/reduce_scatter | solution.py:409
  (8 shorter events, 0.1 us)
Async XLA Ops:
  6.5 138.0 %reduce-scatter.2.cloned.1.call-start = ((), (), s32[]{:S(2)}) async-start(), calls=%async_computation.1 | async-start | bytes 6553600 | tf_op jit(solution)/shard_map/reduce_scatter | solution.py:409
Sparse Core Ops, SparseCore 0:
  74.9 69.6 reduce-scatter.1

commit v2 on v1

--- a/solution.py
+++ b/solution.py
@@ -18,6 +18,7 @@
 GROUP = 4
 SPANS = 20
 WIDTH = 512
+OUT_ROWS = 160
 D = 4096
 CHUNK = 1024
 KV = ("kv_0", "kv_1", "kv_2")
@@ -34,6 +35,40 @@
 
 def nn_dot(a, b):
     return jnp.dot(a, b, preferred_element_type=F32)
+
+
+def make_plan(chosen_ref, need_ref, bias_ref):
+    lane = lax.broadcasted_iota(jnp.int32, (BLOCKS, N_SEL), 1)
+    spread = lax.broadcasted_iota(jnp.int32, (N_SEL, N_SEL * SB), 1) // SB
+    spread = spread == lax.broadcasted_iota(jnp.int32, (N_SEL, N_SEL * SB), 0)
+    spread = jnp.where(spread, 1.0, 0.0).astype(BF16)
+    need_lane = lax.broadcasted_iota(jnp.int32, (1, 128), 1)
+    named = [chosen_ref[:, g, :] for g in range(GROUPS)]
+    for g in range(GROUPS):
+        repeated = jnp.zeros((BLOCKS, N_SEL), F32)
+        for t in range(N_SEL - 1):
+            same = jnp.logical_and(named[g] == named[g][:, t : t + 1], lane > t)
+            repeated = jnp.where(same, 1.0, repeated)
+        bias = nn_dot(repeated.astype(BF16), spread) * LOW
+        for b in range(BLOCKS):
+            bias_ref[g, b] = bias[b : b + 1]
+    places = [n - (n // BLOCKS) * BLOCKS for n in named]
+    sources = [n // BLOCKS for n in named]
+
+    def ends(axis_min, value):
+        for axis in (0, 1):
+            value = axis_min(value, axis=axis, keepdims=True)
+        return value
+
+    for s in range(N_KV):
+        row = jnp.zeros((1, 128), jnp.int32)
+        for g in range(GROUPS):
+            hit = sources[g] == s
+            first = ends(jnp.min, jnp.where(hit, places[g], BLOCKS - 1))
+            last = ends(jnp.max, jnp.where(hit, places[g], 0))
+            row = jnp.where(need_lane == 2 * g, first, row)
+            row = jnp.where(need_lane == 2 * g + 1, last, row)
+        need_ref[s] = row
 
 
 def body(
@@ -45,9 +80,9 @@
     pos_ref,
     kmix_ref,
     vmix_ref,
-    need_ref,
-    idx_ref,
-    bias_ref,
+    wo_hbm,
+    chosen_ref,
+    chosen_s,
     out_ref,
     tok,
     wq,
@@ -63,8 +98,19 @@
     stage,
     mine,
     comp,
+    need_ref,
+    need_s,
+    bias_ref,
+    wall,
+    att,
+    got,
+    total_ref,
     load_sem,
     asked_sem,
+    w_send,
+    w_recv,
+    att_send,
+    att_recv,
     need_send,
     need_recv,
     sum_send,
@@ -78,7 +124,10 @@
     def at(d):
         return (d // 8, lax.rem(d // 2, 4), lax.rem(d, 2), x)
 
+    left, right, far = (lax.rem(x + hop, N_TP) for hop in (3, 1, 2))
     barrier = pltpu.get_barrier_semaphore()
+    for peer in (left, right, far):
+        pl.semaphore_signal(barrier, inc=1, device_id=(kz, ky, kc, peer), device_id_type=MESH)
 
     def greet(d, carry):
         @pl.when(d != me)
@@ -109,13 +158,64 @@
         )
     wg_load = load(wg_hbm, wg)
     wq_load = load(wq_hbm, wq)
+    wo_load = load(wo_hbm, wall.at[pl.ds(pl.multiple_of(x * WIDTH, WIDTH), WIDTH)])
+    make_plan(chosen_ref, need_ref, bias_ref)
+    need_load = pltpu.make_async_copy(need_ref, need_s, load_sem.at[15])
+    need_load.start()
 
     def clear(d, carry):
         sums[d] = jnp.zeros(sums.shape[1:], BF16)
         return carry
 
     lax.fori_loop(me + 1, N_KV, clear, 0)
-    pl.semaphore_wait(barrier, N_KV - 1)
+    pl.semaphore_wait(barrier, N_KV - 1 + N_TP - 1)
+
+    color = lax.rem(ky + kz, 2)
+    mine_row = color * 256 + kc * 128
+    other_row = (1 - color) * 256 + kc * 128
+
+    def region(shard, row, count):
+        return wall.at[pl.ds(pl.multiple_of(shard * WIDTH + row, 32), count)]
+
+    def w_copy(index, src, dst, device):
+        return pltpu.make_async_remote_copy(
+            src_ref=src,
+            dst_ref=dst,
+            send_sem=w_send.at[index],
+            recv_sem=w_recv.at[index],
+            device_id=device,
+            device_id_type=MESH,
+        )
+
+    def w_first(index, shard, receiving=False):
+        to_right = index in (0, 1, 4)
+        row = mine_row + (64 if index in (1, 2, 5) else 0)
+        src = region(shard, row, 64)
+        if index < 4 and not receiving:
+            src = wo_hbm.at[pl.ds(pl.multiple_of(row, 32), 64)]
+        device = (kz, ky, kc, right if to_right else left)
+        return w_copy(index, src, region(shard, row, 64), device)
+
+    directions = (
+        (kz, lax.rem(ky + 1, 4), kc, x),
+        (kz, lax.rem(ky + 3, 4), kc, x),
+        (lax.rem(kz + 1, 4), ky, kc, x),
+        (lax.rem(kz + 3, 4), ky, kc, x),
+    )
+    shards = (left, right, far)
+
+    def w_second(j, o, receiving=False):
+        part = region(shards[o], (other_row if receiving else mine_row) + 32 * j, 32)
+        return w_copy(6 + 3 * j + o, part, part, directions[j])
+
+    def w_third(half, o, receiving=False):
+        row = mine_row if half == 0 else other_row
+        row = row - kc * 128 + (1 - kc) * 128 if receiving else row
+        part = region(shards[o], row, 128)
+        return w_copy(18 + 3 * half + o, part, part, (kz, ky, 1 - kc, x))
+
+    for index in (0, 2, 1, 3):
+        w_first(index, x).start()
 
     def need_copy(d, sender):
         return pltpu.make_async_remote_copy(
@@ -148,16 +248,22 @@
     offsets = pos_ref[...].astype(F32)
     offsets = jnp.concatenate([offsets, offsets], axis=1)
     lane_low = lax.broadcasted_iota(jnp.int32, (CMP, 128), 1) < HD
-    lane_head = lax.broadcasted_iota(jnp.int32, (CMP, 8), 1)
+    row_head = lax.broadcasted_iota(jnp.int32, (8, CMP), 0)
+    diagonal = lax.broadcasted_iota(jnp.int32, (CMP, CMP), 0) == lax.broadcasted_iota(
+        jnp.int32, (CMP, CMP), 1
+    )
+
+    def column(ref, head):
+        row = jnp.sum(jnp.where(row_head == head, ref[...].astype(F32), 0.0), axis=0, keepdims=True)
+        return jnp.sum(jnp.where(diagonal, row, 0.0), axis=1, keepdims=True)
+
     for g in range(GROUPS):
         pair = pairs[g]
         blocks = pair.astype(BF16).reshape(BLOCKS, SB, 128)
         mine[g] = blocks
         table[4 * N_KV + g * BLOCKS : 4 * N_KV + (g + 1) * BLOCKS] = blocks
-        own = lane_head == x * GROUPS + g
-        kmix = jnp.sum(jnp.where(own, kmix_ref[...].astype(F32), 0.0), axis=1, keepdims=True)
-        vmix = jnp.sum(jnp.where(own, vmix_ref[...].astype(F32), 0.0), axis=1, keepdims=True)
-        mixing = jnp.where(lane_low, kmix, vmix)
+        head = x * GROUPS + g
+        mixing = jnp.where(lane_low, column(kmix_ref, head), column(vmix_ref, head))
         spans = jnp.sum((pair.reshape(SPANS, CMP, 128) + offsets[None]) * mixing[None], axis=1)
         sums[me, 0, g] = spans[:16].astype(BF16)
         sums[me, 1, g] = jnp.concatenate([spans[16:], jnp.zeros((12, 128), F32)], axis=0).astype(
@@ -222,11 +328,16 @@
             tile = jnp.where(low, tile, 0.0).astype(BF16) * BF16(HD**-0.5)
             qp[:, g, r] = tile.reshape(BLOCKS, SB, 128)
     wg_load.wait()
-    pick = lax.broadcasted_iota(jnp.int32, (64, 128), 0) == (
-        lax.broadcasted_iota(jnp.int32, (64, 128), 1) + x * 16
+    pick = lax.broadcasted_iota(jnp.int32, (128, 64), 1) == (
+        lax.broadcasted_iota(jnp.int32, (128, 64), 0) + x * 16
     )
-    own_gates = nn_dot(wg[...], jnp.where(pick, 1.0, 0.0).astype(BF16)).astype(BF16)
-    gates[...] = jax.nn.sigmoid(nn_dot(tok[...], own_gates)).reshape(BLOCKS, SB, 128)
+    own_gates = nn_dot(jnp.where(pick, 1.0, 0.0).astype(BF16), wg[...]).astype(BF16)
+    gates[...] = jax.nn.sigmoid(nt_dot(tok[...], own_gates)).reshape(BLOCKS, SB, 128)
+
+    w_first(0, left, True).wait_recv()
+    w_first(4, left).start()
+    w_first(2, right, True).wait_recv()
+    w_first(5, right).start()
 
     def take_sum(s, carry):
         sum_copy(me, s).wait_recv()
@@ -283,12 +394,42 @@
     causal = jnp.logical_or(lane_first >= SB, lane_first <= row_b)
     low_half = lax.broadcasted_iota(jnp.int32, (SB, 128), 1) < HD
 
-    def chosen_block(b, carry):
+    need_load.wait()
+    for index, shard in ((1, left), (3, right), (4, far), (5, far)):
+        w_first(index, shard, True).wait_recv()
+    for o in range(3):
+        for j in range(4):
+            w_second(j, o).start()
+    for o in range(3):
+        w_third(0, o).start()
+
+    def att_copy(target, sender):
+        return pltpu.make_async_remote_copy(
+            src_ref=att.at[pl.ds(pl.multiple_of(target * OUT_ROWS, 32), OUT_ROWS)],
+            dst_ref=got.at[sender],
+            send_sem=att_send.at[target],
+            recv_sem=att_recv.at[sender],
+            device_id=(kz, ky, kc, target),
+            device_id_type=MESH,
+        )
+
+    first_block = lax.rem(5 * (x + 1) // 2, BLOCKS)
+
+    def chosen_block(i, carry):
+        b = lax.rem(first_block + i, BLOCKS)
         for g in range(GROUPS):
             q = qp[b, g].reshape(GROUP * SB, 128)
-            base = (b * GROUPS + g) * N_SEL
-            picked = jnp.concatenate([table[idx_ref[base + s]] for s in range(N_SEL)], axis=0)
-            score = nt_dot(q, picked) + bias_ref[b * GROUPS + g]
+            pieces = []
+            for s in range(N_SEL):
+                named = chosen_s[b, g, s]
+                source = named // BLOCKS
+                place = named - source * BLOCKS
+                second = (place != need_s[source, 0, 2 * g]).astype(jnp.int32)
+                away = (source * GROUPS + g) * 2 + second
+                home = 4 * N_KV + g * BLOCKS + place
+                pieces.append(table[jnp.where(source == me, home, away)])
+            picked = jnp.concatenate(pieces, axis=0)
+            score = nt_dot(q, picked) + bias_ref[g, b]
             head = jnp.where(causal, score[:, :128], LOW)
             score = jnp.concatenate([head, score[:, 128:]], axis=1)
             most = jnp.max(score, axis=1, keepdims=True)
@@ -301,10 +442,55 @@
                 odd = both[(2 * half + 1) * SB : (2 * half + 2) * SB]
                 tile = jnp.where(low_half, pltpu.roll(even, HD, 1), odd).astype(BF16)
                 lanes = slice(256 * g + 128 * half, 256 * g + 128 * half + 128)
-                out_ref[pl.ds(pl.multiple_of(b * SB, SB), SB), lanes] = tile
+                att[pl.ds(pl.multiple_of(b * SB, SB), SB), lanes] = tile
+        for hop, last in ((1, 2), (2, 5), (3, 7)):
+
+            @pl.when(i == last)
+            def _():
+                target = lax.rem(x + hop, N_TP)
+                att_copy(target, x).start()
+
         return carry
 
     lax.fori_loop(0, BLOCKS, chosen_block, 0)
+    for o in range(3):
+        for j in range(4):
+            w_second(j, o, True).wait_recv()
+        w_third(1, o).start()
+
+    wo_load.wait()
+    got[x] = att[pl.ds(pl.multiple_of(x * OUT_ROWS, 32), OUT_ROWS)]
+    for order, shard in enumerate((x, left, right, far)):
+        if order:
+            att_copy(shard, shard).wait_recv()
+            w_third(0, order - 1, True).wait_recv()
+            w_third(1, order - 1, True).wait_recv()
+
+        def project(n, carry):
+            cols = pl.ds(pl.multiple_of(n * 256, 256), 256)
+            rows = pl.ds(pl.multiple_of(shard * WIDTH, WIDTH), WIDTH)
+            part = nn_dot(got[shard], wall[rows, cols])
+            if order:
+                part = part + total_ref[:, cols]
+            if order < 3:
+                total_ref[:, cols] = part
+            else:
+                out_ref[:, cols] = part.astype(BF16)
+            return carry
+
+        lax.fori_loop(0, D // 256, project, 0)
+
+    for index in (0, 1, 2, 3):
+        w_first(index, x).wait_send()
+    w_first(4, left).wait_send()
+    w_first(5, right).wait_send()
+    for o in range(3):
+        for j in range(4):
+            w_second(j, o).wait_send()
+        w_third(0, o).wait_send()
+        w_third(1, o).wait_send()
+    for hop in (1, 2, 3):
+        att_copy(lax.rem(x + hop, N_TP), x).wait_send()
 
     def sent_need(d, carry):
         need_copy(d, me).wait_send()
@@ -318,30 +504,6 @@
         return carry
 
     lax.fori_loop(me + 1, N_KV, sent_rest, 0)
-
-
-def plan(chosen, me):
-    named = chosen.transpose(1, 0, 2).reshape(GROUPS, BLOCKS * N_SEL)
-    source = named // BLOCKS
-    place = named - source * BLOCKS
-    hit = source[:, None, :] == jnp.arange(N_KV, dtype=jnp.int32)[None, :, None]
-    first = jnp.min(jnp.where(hit, place[:, None, :], BLOCKS), axis=2)
-    last = jnp.max(jnp.where(hit, place[:, None, :], 0), axis=2)
-    first_there = jnp.sum(jnp.where(hit, first[:, :, None], 0), axis=1)
-    first = jnp.where(first == BLOCKS, 0, first)
-    group = jnp.arange(GROUPS, dtype=jnp.int32)[:, None]
-    far = (source * GROUPS + group) * 2 + (place != first_there).astype(jnp.int32)
-    near = 4 * N_KV + group * BLOCKS + place
-    index = jnp.where(source == me, near, far)
-    index = index.reshape(GROUPS, BLOCKS, N_SEL).transpose(1, 0, 2).reshape(-1)
-    need = jnp.stack([first, last], axis=-1).transpose(1, 0, 2).reshape(N_KV, 1, 2 * GROUPS)
-    need = jnp.pad(need, ((0, 0), (0, 0), (0, 128 - 2 * GROUPS)))
-    same = chosen[..., :, None] == chosen[..., None, :]
-    slot = jnp.arange(N_SEL, dtype=jnp.int32)
-    repeated = jnp.any(same & (slot[None, :] < slot[:, None]), axis=-1)
-    bias = jnp.where(repeated, LOW, 0.0).astype(F32)
-    bias = jnp.repeat(bias, SB, axis=-1).reshape(BLOCKS * GROUPS, 1, N_SEL * SB)
-    return need, index, bias
 
 
 def local(
@@ -356,21 +518,20 @@
     out_weight,
     chosen,
 ):
-    need, index, bias = plan(chosen, lax.axis_index(KV))
     any_space = pl.BlockSpec(memory_space=pl.ANY)
     vmem = pl.BlockSpec(memory_space=pltpu.VMEM)
     smem = pl.BlockSpec(memory_space=pltpu.SMEM)
     dma = pltpu.SemaphoreType.DMA
-    attention = pl.pallas_call(
+    return pl.pallas_call(
         body,
-        out_shape=jax.ShapeDtypeStruct((ROWS, WIDTH), BF16),
-        in_specs=[any_space] * 5 + [vmem] * 4 + [smem, vmem],
+        out_shape=jax.ShapeDtypeStruct((OUT_ROWS, D), BF16),
+        in_specs=[any_space] * 5 + [vmem] * 3 + [any_space, vmem, smem],
         out_specs=vmem,
         scratch_shapes=[
             pltpu.VMEM((ROWS, D), BF16),
             pltpu.VMEM((D, WIDTH), BF16),
             pltpu.VMEM((D, 256), BF16),
-            pltpu.VMEM((D, 64), BF16),
+            pltpu.VMEM((64, D), BF16),
             pltpu.VMEM((ROWS, 256), F32),
             pltpu.VMEM((BLOCKS, SB, 128), F32),
             pltpu.VMEM((BLOCKS, GROUPS, GROUP, SB, 128), BF16),
@@ -381,8 +542,19 @@
             pltpu.VMEM((N_KV, 4, SB, 128), BF16),
             pltpu.VMEM((GROUPS, BLOCKS, SB, 128), BF16),
             pltpu.VMEM((BLOCKS, GROUPS, GROUP * SB, 128), F32),
+            pltpu.VMEM((N_KV, 1, 128), jnp.int32),
+            pltpu.SMEM((N_KV, 1, 128), jnp.int32),
+            pltpu.VMEM((GROUPS, BLOCKS, 1, N_SEL * SB), F32),
+            pltpu.VMEM((N_TP * WIDTH, D), BF16),
+            pltpu.VMEM((ROWS, WIDTH), BF16),
+            pltpu.VMEM((N_TP, OUT_ROWS, WIDTH), BF16),
+            pltpu.VMEM((OUT_ROWS, D), F32),
             dma((16,)),
             dma((N_KV,)),
+            dma((24,)),
+            dma((24,)),
+            dma((N_TP,)),
+            dma((N_TP,)),
             dma((N_KV,)),
             dma((N_KV,)),
             dma((N_KV,)),
@@ -398,19 +570,13 @@
         query_weight,
         key_weight,
         value_weight,
-        gate_weight,
+        gate_weight.T,
         summary_pos,
-        key_mixing,
-        value_mixing,
-        need,
-        index,
-        bias,
-    )
-    return lax.psum_scatter(
-        jnp.dot(attention, out_weight, preferred_element_type=F32).astype(BF16),
-        "tp",
-        scatter_dimension=0,
-        tiled=True,
+        key_mixing.T,
+        value_mixing.T,
+        out_weight,
+        chosen,
+        chosen,
     )
 
 

time: 152 us -> 88.3 us (0.58)
  waiting for transfers between devices: 69.8 us -> 0 us
  Pallas kernels: 50 us -> 85.6 us
  between operations: 13.4 us -> 0.01 us
  matrix products: 7.59 us -> 0 us
  local copies, waits for them, and re-layouts: 8.19 us -> 2.49 us
  other arithmetic: 2.36 us -> 0 us
    reduce_scatter x1 -> x0, waiting for transfers between devices: 69.8 us -> none  [local(): lax.psum_scatter(jnp.dot(attention, out_weight, preferred_element_type=F3...]
    pallas_call x1, Pallas kernels: 50 us -> 85.6 us  [local(): pl.pallas_call(body, out_shape=jax.ShapeDtypeStruct((OUT_ROWS, D), BF16),...]
    dot_general x1 -> x0, matrix products: 7.59 us -> none  [local(): jnp.dot(attention, out_weight, preferred_element_type=F32).astype(BF16)]
    unnamed x4 -> x1, local copies, waits for them, and re-layouts: 5.77 us -> 2.49 us
  transfers between devices with their start and end apart: 1 -> 0, of which waited for: 1 -> 0; matrix products, arithmetic and copies ran while one was open for 0% -> 0% of each run, Pallas kernels for 0% -> 0%
where the time goes in v2:
time: 88.3 us; the launch traced here: 88.1 us
  Pallas kernels  85.6 us (97%)
  local copies, waits for them, and re-layouts  2.49 us (3%)
    pallas_call x1, Pallas kernels, local(): pl.pallas_call(body, out_shape=jax.ShapeDtypeStruct((OUT_ROWS, D), BF16),...  85.6 us
    unnamed x1, local copies, waits for them, and re-layouts  2.49 us

profile of v2, /device:TPU:1, one launch (start us, length us, event | category | flops | bytes accessed | tf_op | source)
XLA Modules:
  0.0 88.1 jit_solution(1253405315052717109)
XLA Ops:
  0.0 85.6 %shard_map.100 = bf16[160,4096]{1,0:T(8,128)(2,1)} custom-call(bf16[640,4096]{1,0:T(8,128)(2,1)} %tok_hbm.1, bf16[4096,512]{1,0:T(8,128)(2,1)} %wq_hbm.1, bf16[4096,128]{1,0:T(8,128)(2,1)} %wk_hbm.1, bf16[4096,128]{1,0:T(8,128)(2,1)} %wv_hbm.1, bf16[64,4096]{1,0:T(8,128)(2,1)} %bitcast.3, bf16[32,64]{1,0:T(8,128)(2,1)} %pos_ref.1, bf16[8,32]{1,0:T(8,128)(2,1)} %bitcast.4, ...), custom_call_target="tpu_custom_call" | custom-call | tf_op jit(solution)/shard_map/pallas_call | solution.py:525
  85.6 2.5 %copy.12 = bf16[160,4096]{1,0:T(8,128)(2,1)} copy(bf16[160,4096]{1,0:T(8,128)(2,1)} %shard_map.100) | data formatting | bytes 2621440

commit v3 on v2

v3 whole, which is shorter than its diff:
```python
import jax
import jax.numpy as jnp
from jax import lax
from jax.experimental import pallas as pl
from jax.experimental.pallas import tpu as pltpu
from jax.sharding import Mesh
from jax.sharding import PartitionSpec as P

HD = 64
CMP = 32
SB = 64
N_SEL = 16
N_KV = 32
N_Z = 4
PLANE = 8
N_TP = 4
ROWS = 640
BLOCKS = 10
GROUPS = 2
GROUP = 4
SPANS = 20
WIDTH = 512
OUT_ROWS = 160
D = 4096
CHUNK = 1024
KV = ("kv_0", "kv_1", "kv_2")
KV_TP = ("kv_0", "kv_1", "kv_2", "tp")
MESH = pl.DeviceIdType.MESH
BF16 = jnp.bfloat16
F32 = jnp.float32
LOW = -1e30


def nt_dot(a, b):
    return lax.dot_general(a, b, (((1,), (1,)), ((), ())), preferred_element_type=F32)


def nn_dot(a, b):
    return jnp.dot(a, b, preferred_element_type=F32)


def make_plan(chosen_ref, need_ref, bias_ref):
    lane = lax.broadcasted_iota(jnp.int32, (BLOCKS, N_SEL), 1)
    spread = lax.broadcasted_iota(jnp.int32, (N_SEL, N_SEL * SB), 1) // SB
    spread = spread == lax.broadcasted_iota(jnp.int32, (N_SEL, N_SEL * SB), 0)
    spread = jnp.where(spread, 1.0, 0.0).astype(BF16)
    need_lane = lax.broadcasted_iota(jnp.int32, (1, 128), 1)
    named = [chosen_ref[:, g, :] for g in range(GROUPS)]
    for g in range(GROUPS):
        repeated = jnp.zeros((BLOCKS, N_SEL), F32)
        for t in range(N_SEL - 1):
            same = jnp.logical_and(named[g] == named[g][:, t : t + 1], lane > t)
            repeated = jnp.where(same, 1.0, repeated)
        bias = nn_dot(repeated.astype(BF16), spread) * LOW
        for b in range(BLOCKS):
            bias_ref[g, b] = bias[b : b + 1]
    places = [n - (n // BLOCKS) * BLOCKS for n in named]
    sources = [n // BLOCKS for n in named]

    def ends(axis_min, value):
        for axis in (0, 1):
            value = axis_min(value, axis=axis, keepdims=True)
        return value

    for s in range(N_KV):
        row = jnp.zeros((1, 128), jnp.int32)
        for g in range(GROUPS):
            hit = sources[g] == s
            first = ends(jnp.min, jnp.where(hit, places[g], BLOCKS - 1))
            last = ends(jnp.max, jnp.where(hit, places[g], 0))
            row = jnp.where(need_lane == 2 * g, first, row)
            row = jnp.where(need_lane == 2 * g + 1, last, row)
        need_ref[s // PLANE, s % PLANE] = row


def body(
    tok_hbm,
    wq_hbm,
    wk_hbm,
    wv_hbm,
    wg_hbm,
    pos_ref,
    kmix_ref,
    vmix_ref,
    wo_hbm,
    chosen_ref,
    chosen_s,
    out_ref,
    tok,
    wq,
    wkv,
    wg,
    acc,
    gates,
    qp,
    sums,
    asked,
    asked_s,
    table,
    stage,
    unit_0,
    unit_1,
    unit_2,
    unit_3,
    comp,
    need_ref,
    need_s,
    bias_ref,
    wall,
    att,
    got,
    load_sem,
    asked_sem,
    w_send,
    w_recv,
    att_send,
    att_recv,
    need_send,
    need_recv,
    lift_send,
    lift_recv,
    unit_send,
    unit_recv,
    sum_send,
    sum_recv,
    blk_send,
    blk_recv,
):
    kz, ky, kc, x = (lax.axis_index(name) for name in KV_TP)
    kp = ky * 2 + kc
    me = kz * PLANE + kp
    units = (unit_0, unit_1, unit_2, unit_3)

    def in_plane(p):
        return (kz, p // 2, lax.rem(p, 2), x)

    def above(hops):
        return (lax.rem(kz + hops, N_Z), ky, kc, x)

    left, right, far = (lax.rem(x + hop, N_TP) for hop in (3, 1, 2))
    barrier = pltpu.get_barrier_semaphore()

    def signal(device):
        pl.semaphore_signal(barrier, inc=1, device_id=device, device_id_type=MESH)

    for peer in (left, right, far):
        signal((kz, ky, kc, peer))
    for hops in (1, 2, 3):
        signal(above(hops))
    for hop in range(1, PLANE):
        signal(in_plane(lax.rem(kp + hop, PLANE)))

    loads = []

    def load(src, dst):
        loads.append(pltpu.make_async_copy(src, dst, load_sem.at[len(loads)]))
        loads[-1].start()
        return loads[-1]

    steps = D // CHUNK
    kv_loads = []
    for k in range(steps):
        rows = pl.ds(k * CHUNK, CHUNK)
        kv_loads.append(
            (
                load(wk_hbm.at[rows], wkv.at[rows, pl.ds(0, 128)]),
                load(wv_hbm.at[rows], wkv.at[rows, pl.ds(128, 128)]),
                load(tok_hbm.at[:, rows], tok.at[:, rows]),
            )
        )
    wq_load = load(wq_hbm, wq)
    wg_load = load(wg_hbm, wg.at[pl.ds(0, 64)])
    wo_load = load(wo_hbm, wall.at[pl.ds(pl.multiple_of(x * WIDTH, WIDTH), WIDTH)])
    with jax.named_scope("plan"):
        make_plan(chosen_ref, need_ref, bias_ref)
        need_load = pltpu.make_async_copy(need_ref, need_s, load_sem.at[15])
        need_load.start()
    wg[64:] = jnp.zeros((64, D), BF16)

    def clear(d, carry):
        sums[d // PLANE, lax.rem(d, PLANE)] = jnp.zeros(sums.shape[2:], BF16)
        return carry

    lax.fori_loop(me + 1, N_KV, clear, 0)
    with jax.named_scope("barrier_wait"):
        pl.semaphore_wait(barrier, PLANE - 1 + N_Z - 1 + N_TP - 1)

    def remote(src, dst, send, recv, device):
        return pltpu.make_async_remote_copy(
            src_ref=src,
            dst_ref=dst,
            send_sem=send,
            recv_sem=recv,
            device_id=device,
            device_id_type=MESH,
        )

    def need_copy(p, sender):
        return remote(
            need_ref.at[:, p], asked.at[sender], need_send.at[p], need_recv.at[sender], in_plane(p)
        )

    def peers(fn):
        def step(p, carry):
            @pl.when(p != kp)
            def _():
                fn(p)

            return carry

        lax.fori_loop(0, PLANE, step, 0)

    peers(lambda p: need_copy(p, kp).start())

    color = lax.rem(ky + kz, 2)
    mine_row = color * 256 + kc * 128
    other_row = (1 - color) * 256 + kc * 128

    def region(shard, row, count):
        return wall.at[pl.ds(pl.multiple_of(shard * WIDTH + row, 32), count)]

    def w_copy(index, src, dst, device):
        return remote(src, dst, w_send.at[index], w_recv.at[index], device)

    def w_first(index, shard, receiving=False):
        to_right = index in (0, 1, 4)
        row = mine_row + (64 if index in (1, 2, 5) else 0)
        src = region(shard, row, 64)
        if index < 4 and not receiving:
            src = wo_hbm.at[pl.ds(pl.multiple_of(row, 32), 64)]
        device = (kz, ky, kc, right if to_right else left)
        return w_copy(index, src, region(shard, row, 64), device)

    directions = (
        (kz, lax.rem(ky + 1, 4), kc, x),
        (kz, lax.rem(ky + 3, 4), kc, x),
        (lax.rem(kz + 1, 4), ky, kc, x),
        (lax.rem(kz + 3, 4), ky, kc, x),
    )
    shards = (left, right, far)

    def w_second(j, o, receiving=False):
        part = region(shards[o], (other_row if receiving else mine_row) + 32 * j, 32)
        return w_copy(6 + 3 * j + o, part, part, directions[j])

    def w_third(half, o, receiving=False):
        row = mine_row if half == 0 else other_row
        row = row - kc * 128 + (1 - kc) * 128 if receiving else row
        part = region(shards[o], row, 128)
        return w_copy(18 + 3 * half + o, part, part, (kz, ky, 1 - kc, x))

    for index in (0, 2, 1, 3):
        w_first(index, x).start()

    with jax.named_scope("kv_proj"):
        for k in range(steps):
            for copy in kv_loads[k]:
                copy.wait()
            part = nn_dot(tok[:, k * CHUNK : (k + 1) * CHUNK], wkv[k * CHUNK : (k + 1) * CHUNK])
            acc[...] = part if k == 0 else acc[...] + part
    low = lax.broadcasted_iota(jnp.int32, (ROWS, 128), 1) < HD
    keys = acc[:, :128].astype(BF16).astype(F32)
    values = acc[:, 128:].astype(BF16).astype(F32)
    pairs = (
        jnp.where(low, keys, pltpu.roll(values, HD, 1)),
        jnp.where(low, pltpu.roll(keys, HD, 1), values),
    )
    offsets = pos_ref[...].astype(F32)
    offsets = jnp.concatenate([offsets, offsets], axis=1)
    lane_low = lax.broadcasted_iota(jnp.int32, (CMP, 128), 1) < HD
    row_head = lax.broadcasted_iota(jnp.int32, (8, CMP), 0)
    diagonal = lax.broadcasted_iota(jnp.int32, (CMP, CMP), 0) == lax.broadcasted_iota(
        jnp.int32, (CMP, CMP), 1
    )

    def column(ref, head):
        row = jnp.sum(jnp.where(row_head == head, ref[...].astype(F32), 0.0), axis=0, keepdims=True)
        return jnp.sum(jnp.where(diagonal, row, 0.0), axis=1, keepdims=True)

    with jax.named_scope("summary"):
        tails = []
        for g in range(GROUPS):
            pair = pairs[g]
            blocks = pair.astype(BF16).reshape(BLOCKS, SB, 128)
            unit_0[g] = blocks
            table[4 * N_KV + g * BLOCKS : 4 * N_KV + (g + 1) * BLOCKS] = blocks
            head = x * GROUPS + g
            mixing = jnp.where(lane_low, column(kmix_ref, head), column(vmix_ref, head))
            spans = jnp.sum((pair.reshape(SPANS, CMP, 128) + offsets[None]) * mixing[None], axis=1)
            sums[kz, kp, 16 * g : 16 * g + 16] = spans[:16].astype(BF16)
            tails.append(spans[16:])
        sums[kz, kp, 32:] = jnp.concatenate(tails, axis=0).astype(BF16)

    def lift_copy(hops, receiving=False):
        part = sums.at[kz - hops if receiving else kz, kp]
        return remote(part, part, lift_send.at[hops], lift_recv.at[hops], above(hops))

    def sum_copy(hops, p, sender):
        part = sums.at[kz - hops, sender]
        k = hops * PLANE
        return remote(part, part, sum_send.at[k + p], sum_recv.at[k + sender], in_plane(p))

    def spread(hops, fn):
        def step(p, carry):
            @pl.when(p > kp if hops == 0 else p != kp)
            def _():
                fn(p)

            return carry

        lax.fori_loop(0, PLANE, step, 0)

    def arriving(hops, fn):
        def step(p, carry):
            @pl.when(p < kp if hops == 0 else p != kp)
            def _():
                fn(p)

            return carry

        lax.fori_loop(0, PLANE, step, 0)

    for hops in (1, 2, 3):

        @pl.when(kz + hops < N_Z)
        def _():
            lift_copy(hops).start()

    spread(0, lambda p: sum_copy(0, p, kp).start())

    def unit_copy(hops):
        src = unit_0 if hops in (1, 3) else unit_1
        device = above(3 if hops == 3 else 1)
        return remote(src, units[hops], unit_send.at[hops], unit_recv.at[hops], device)

    sends_unit = {1: kz < 3, 2: jnp.logical_or(kz == 1, kz == 2), 3: kz == 0}
    for hops in (1, 3):

        @pl.when(sends_unit[hops])
        def _():
            unit_copy(hops).start()

    with jax.named_scope("need_wait"):

        def take_need(p):
            need_copy(kp, p).wait_recv()
            pltpu.make_async_copy(asked.at[p], asked_s.at[p], asked_sem.at[p]).start()

        peers(take_need)
        peers(lambda p: pltpu.make_async_copy(asked.at[p], asked_s.at[p], asked_sem.at[p]).wait())
        need_load.wait()

    def blk_copy(hops, p, sender):
        dst = table.at[pl.ds(((kz - hops) * PLANE + sender) * 4, 4)]
        k = hops * PLANE
        return remote(
            stage.at[hops, p], dst, blk_send.at[k + p], blk_recv.at[k + sender], in_plane(p)
        )

    def serve(hops):
        @pl.when(kz >= hops)
        def _():
            if hops:
                unit_copy(hops).wait_recv()
            if hops == 1:

                @pl.when(sends_unit[2])
                def _():
                    unit_copy(2).start()

            def one(p):
                for slot in range(4):
                    block = asked_s[p, kz - hops, 0, slot]
                    stage[hops, p, slot] = units[hops][slot // 2, block]
                blk_copy(hops, p, kp).start()

            spread(hops, one)
            if hops:
                for slot in range(4):
                    block = need_s[kz - hops, kp, 0, slot]
                    place = ((kz - hops) * PLANE + kp) * 4 + slot
                    table[place] = units[hops][slot // 2, block]

    with jax.named_scope("serve_0"):
        serve(0)

    def project_queries(g):
        cols = slice(256 * g, 256 * (g + 1))
        for k in range(steps):
            ks = slice(k * CHUNK, (k + 1) * CHUNK)
            part = nn_dot(tok[:, ks], wq[ks, cols])
            acc[...] = part if k == 0 else acc[...] + part
        for r in range(GROUP):
            tile = acc[:, 128 * (r // 2) : 128 * (r // 2) + 128]
            if r % 2:
                tile = pltpu.roll(tile, HD, 1)
            tile = jnp.where(low, tile, 0.0).astype(BF16) * BF16(HD**-0.5)
            qp[:, g, r] = tile.reshape(BLOCKS, SB, 128)

    with jax.named_scope("q_proj"):
        wq_load.wait()
        project_queries(0)
    with jax.named_scope("sum_pass"):
        for hops in (1, 2, 3):

            @pl.when(kz >= hops)
            def _():
                lift_copy(hops, True).wait_recv()
                spread(hops, lambda p: sum_copy(hops, p, kp).start())

    with jax.named_scope("q_proj"):
        project_queries(1)
    with jax.named_scope("gates"):
        wg_load.wait()
        logits = nt_dot(tok[...], wg[...])
        own = pltpu.roll(logits, lax.rem(128 - x * 16, 128), 1)
        gates[...] = jax.nn.sigmoid(own).reshape(BLOCKS, SB, 128)

    with jax.named_scope("sum_wait"):
        for hops in range(N_Z):

            @pl.when(kz >= hops)
            def _():
                arriving(hops, lambda p: sum_copy(hops, kp, p).wait_recv())

    lane_a = lax.broadcasted_iota(jnp.int32, (GROUP * SB, 512), 1)
    end_a = ((lane_a // 16) * SPANS + lax.rem(lane_a, 16)) * CMP + CMP - 1
    lane_b = lax.broadcasted_iota(jnp.int32, (GROUP * SB, 128), 1)
    end_b = ((lane_b // 4) * SPANS + 16 + lax.rem(lane_b, 4)) * CMP + CMP - 1
    row_a = lax.rem(lax.broadcasted_iota(jnp.int32, (GROUP * SB, 512), 0), SB)
    row_b = lax.rem(lax.broadcasted_iota(jnp.int32, (GROUP * SB, 128), 0), SB)
    row_c = lax.rem(lax.broadcasted_iota(jnp.int32, (GROUP * SB, 1), 0), SB)
    gap_a = end_a - row_a
    gap_b = end_b - row_b

    def gate_cols(b, g, branch):
        cols = [
            gates[b][:, 2 * (GROUP * g + r) + branch : 2 * (GROUP * g + r) + branch + 1]
            for r in range(GROUP)
        ]
        return jnp.concatenate(cols, axis=0)

    span_as = [sums[:, :, 16 * g : 16 * g + 16].reshape(N_KV * 16, 128) for g in range(GROUPS)]
    span_bs = []
    for g in range(GROUPS):
        tails = [
            sums[s // PLANE, s % PLANE, 32:].astype(F32)[4 * g : 4 * g + 4] for s in range(N_KV)
        ]
        span_bs.append(jnp.concatenate(tails, axis=0).astype(BF16))

    def compressed(b, carry):
        start = me * ROWS + b * SB
        for g in range(GROUPS):
            span_a, span_b = span_as[g], span_bs[g]
            q = qp[b, g].reshape(GROUP * SB, 128)
            score_a = jnp.where(gap_a <= start, nt_dot(q, span_a), LOW)
            score_b = jnp.where(gap_b <= start, nt_dot(q, span_b), LOW)
            most = jnp.maximum(
                jnp.max(score_a, axis=1, keepdims=True), jnp.max(score_b, axis=1, keepdims=True)
            )
            prob_a = jnp.exp(score_a - most)
            prob_b = jnp.exp(score_b - most)
            total = jnp.sum(prob_a, axis=1, keepdims=True) + jnp.sum(prob_b, axis=1, keepdims=True)
            mixed = nn_dot(prob_a.astype(BF16), span_a) + nn_dot(prob_b.astype(BF16), span_b)
            sees = row_c + start >= CMP - 1
            factor = jnp.where(sees, gate_cols(b, g, 0) / total, 0.0)
            comp[b, g] = mixed * factor

        @pl.when(b == 0)
        def _():
            with jax.named_scope("serve_1"):
                serve(1)

        @pl.when(b == 1)
        def _():
            with jax.named_scope("relay"):
                w_first(0, left, True).wait_recv()
                w_first(4, left).start()
                w_first(2, right, True).wait_recv()
                w_first(5, right).start()
            with jax.named_scope("serve_3"):
                serve(3)

        @pl.when(b == 6)
        def _():
            with jax.named_scope("serve_2"):
                serve(2)

        return carry

    with jax.named_scope("comp"):
        lax.fori_loop(0, BLOCKS, compressed, 0)

    with jax.named_scope("w1_wait"):
        w_first(1, left, True).wait_recv()
        w_first(3, right, True).wait_recv()
        for o in range(2):
            for j in range(4):
                w_second(j, o).start()
            w_third(0, o).start()
    with jax.named_scope("blk_wait"):
        for hops in range(N_Z):

            @pl.when(kz >= hops)
            def _():
                arriving(hops, lambda p: blk_copy(hops, kp, p).wait_recv())

    lane_first = lax.broadcasted_iota(jnp.int32, (GROUP * SB, 128), 1)
    causal = jnp.logical_or(lane_first >= SB, lane_first <= row_b)
    low_half = lax.broadcasted_iota(jnp.int32, (SB, 128), 1) < HD

    def att_copy(target, sender):
        rows = pl.ds(pl.multiple_of(target * OUT_ROWS, 32), OUT_ROWS)
        return remote(
            att.at[rows],
            got.at[sender],
            att_send.at[target],
            att_recv.at[sender],
            (kz, ky, kc, target),
        )

    first_block = lax.rem(5 * (x + 1) // 2, BLOCKS)

    def chosen_block(i, carry):
        b = lax.rem(first_block + i, BLOCKS)
        for g in range(GROUPS):
            q = qp[b, g].reshape(GROUP * SB, 128)
            pieces = []
            for s in range(N_SEL):
                named = chosen_s[b, g, s]
                source = named // BLOCKS
                place = named - source * BLOCKS
                first = need_s[source // PLANE, lax.rem(source, PLANE), 0, 2 * g]
                away = (source * GROUPS + g) * 2 + (place != first).astype(jnp.int32)
                home = 4 * N_KV + g * BLOCKS + place
                pieces.append(table[jnp.where(source == me, home, away)])
            picked = jnp.concatenate(pieces, axis=0)
            score = nt_dot(q, picked) + bias_ref[g, b]
            head = jnp.where(causal, score[:, :128], LOW)
            score = jnp.concatenate([head, score[:, 128:]], axis=1)
            most = jnp.max(score, axis=1, keepdims=True)
            prob = jnp.exp(score - most)
            total = jnp.sum(prob, axis=1, keepdims=True)
            mixed = nn_dot(prob.astype(BF16), picked)
            both = comp[b, g] + mixed * (gate_cols(b, g, 1) / total)
            for half in range(2):
                even = both[(2 * half) * SB : (2 * half + 1) * SB]
                odd = both[(2 * half + 1) * SB : (2 * half + 2) * SB]
                tile = jnp.where(low_half, pltpu.roll(even, HD, 1), odd).astype(BF16)
                lanes = slice(256 * g + 128 * half, 256 * g + 128 * half + 128)
                att[pl.ds(pl.multiple_of(b * SB, SB), SB), lanes] = tile
        for hop, last in ((1, 2), (2, 5), (3, 7)):

            @pl.when(i == last)
            def _():
                target = lax.rem(x + hop, N_TP)
                att_copy(target, x).start()

        @pl.when(i == 4)
        def _():
            with jax.named_scope("w1_far"):
                w_first(4, far, True).wait_recv()
                w_first(5, far, True).wait_recv()
                for j in range(4):
                    w_second(j, 2).start()
                w_third(0, 2).start()

        @pl.when(i == 8)
        def _():
            with jax.named_scope("w2_near"):
                for o in range(2):
                    for j in range(4):
                        w_second(j, o, True).wait_recv()
                    w_third(1, o).start()

        return carry

    with jax.named_scope("chosen"):
        lax.fori_loop(0, BLOCKS, chosen_block, 0)

    with jax.named_scope("wo_wait"):
        wo_load.wait()
    got[x] = att[pl.ds(pl.multiple_of(x * OUT_ROWS, 32), OUT_ROWS)]
    for order, shard in enumerate((x, left, right, far)):
        if order:
            with jax.named_scope("w3_wait"):
                att_copy(shard, shard).wait_recv()
                w_third(0, order - 1, True).wait_recv()
                w_third(1, order - 1, True).wait_recv()

        def project(n, carry):
            cols = pl.ds(pl.multiple_of(n * CHUNK, CHUNK), CHUNK)
            rows = pl.ds(pl.multiple_of(shard * WIDTH, WIDTH), WIDTH)
            part = nn_dot(got[shard], wall[rows, cols])
            out_ref[:, cols] = part + out_ref[:, cols] if order else part
            return carry

        with jax.named_scope("outproj"):
            lax.fori_loop(0, D // CHUNK, project, 0)
        if order == 0:
            with jax.named_scope("w2_far"):
                for j in range(4):
                    w_second(j, 2, True).wait_recv()
                w_third(1, 2).start()

    with jax.named_scope("drain"):
        peers(lambda p: need_copy(p, kp).wait_send())
        for index in (0, 1, 2, 3):
            w_first(index, x).wait_send()
        w_first(4, left).wait_send()
        w_first(5, right).wait_send()
        for o in range(3):
            for j in range(4):
                w_second(j, o).wait_send()
            w_third(0, o).wait_send()
            w_third(1, o).wait_send()
        for hop in (1, 2, 3):
            att_copy(lax.rem(x + hop, N_TP), x).wait_send()
        for hops in (1, 2, 3):

            @pl.when(kz + hops < N_Z)
            def _():
                lift_copy(hops).wait_send()

            @pl.when(sends_unit[hops])
            def _():
                unit_copy(hops).wait_send()

        for hops in range(N_Z):

            @pl.when(kz >= hops)
            def _():
                def done(p):
                    sum_copy(hops, p, kp).wait_send()
                    blk_copy(hops, p, kp).wait_send()

                spread(hops, done)


def local(
    tokens,
    query_weight,
    key_weight,
    value_weight,
    gate_weight,
    summary_pos,
    key_mixing,
    value_mixing,
    out_weight,
    chosen,
):
    any_space = pl.BlockSpec(memory_space=pl.ANY)
    vmem = pl.BlockSpec(memory_space=pltpu.VMEM)
    smem = pl.BlockSpec(memory_space=pltpu.SMEM)
    dma = pltpu.SemaphoreType.DMA
    unit = pltpu.VMEM((GROUPS, BLOCKS, SB, 128), BF16)
    requests = (N_Z, PLANE, 1, 128)
    total = pl.pallas_call(
        body,
        out_shape=jax.ShapeDtypeStruct((OUT_ROWS, D), F32),
        in_specs=[any_space] * 5 + [vmem] * 3 + [any_space, vmem, smem],
        out_specs=vmem,
        scratch_shapes=[
            pltpu.VMEM((ROWS, D), BF16),
            pltpu.VMEM((D, WIDTH), BF16),
            pltpu.VMEM((D, 256), BF16),
            pltpu.VMEM((128, D), BF16),
            pltpu.VMEM((ROWS, 256), F32),
            pltpu.VMEM((BLOCKS, SB, 128), F32),
            pltpu.VMEM((BLOCKS, GROUPS, GROUP, SB, 128), BF16),
            pltpu.VMEM((N_Z, PLANE, 40, 128), BF16),
            pltpu.VMEM((PLANE, N_Z, 1, 128), jnp.int32),
            pltpu.SMEM((PLANE, N_Z, 1, 128), jnp.int32),
            pltpu.VMEM((4 * N_KV + GROUPS * BLOCKS, SB, 128), BF16),
            pltpu.VMEM((N_Z, PLANE, 4, SB, 128), BF16),
            unit,
            unit,
            unit,
            unit,
            pltpu.VMEM((BLOCKS, GROUPS, GROUP * SB, 128), F32),
            pltpu.VMEM(requests, jnp.int32),
            pltpu.SMEM(requests, jnp.int32),
            pltpu.VMEM((GROUPS, BLOCKS, 1, N_SEL * SB), F32),
            pltpu.VMEM((N_TP * WIDTH, D), BF16),
            pltpu.VMEM((ROWS, WIDTH), BF16),
            pltpu.VMEM((N_TP, OUT_ROWS, WIDTH), BF16),
            dma((16,)),
            dma((PLANE,)),
            dma((24,)),
            dma((24,)),
            dma((N_TP,)),
            dma((N_TP,)),
            dma((PLANE,)),
            dma((PLANE,)),
            dma((N_Z,)),
            dma((N_Z,)),
            dma((N_Z,)),
            dma((N_Z,)),
            dma((N_KV,)),
            dma((N_KV,)),
            dma((N_KV,)),
            dma((N_KV,)),
        ],
        compiler_params=pltpu.CompilerParams(
            collective_id=0, has_side_effects=True, vmem_limit_bytes=60 * 1024 * 1024
        ),
    )(
        tokens,
        query_weight,
        key_weight,
        value_weight,
        gate_weight.T,
        summary_pos,
        key_mixing.T,
        value_mixing.T,
        out_weight,
        chosen,
        chosen,
    )
    return total.astype(BF16)


def solution(mesh):
    torus = Mesh(mesh.devices.reshape(4, 4, 2, mesh.shape["tp"]), ("kv_0", "kv_1", "kv_2", "tp"))
    in_specs = (
        P(KV, None),
        P(None, "tp"),
        P(None, "tp"),
        P(None, "tp"),
        P(),
        P(),
        P(),
        P(),
        P("tp", None),
        P(KV, "tp", None),
    )
    out_specs = P(KV_TP, None)
    return jax.shard_map(local, mesh=torus, in_specs=in_specs, out_specs=out_specs, check_vma=False)
```

time: 88.3 us -> 71.2 us (0.81)
  Pallas kernels: 85.6 us -> 68 us
  other arithmetic: 0 us -> 2.96 us
  local copies, waits for them, and re-layouts: 2.49 us -> 0 us
    pallas_call x1, Pallas kernels: 85.6 us -> 68 us  [local(): pl.pallas_call(body, out_shape=jax.ShapeDtypeStruct((OUT_ROWS, D), F32),...]
    convert_element_type x0 -> x1, other arithmetic: none -> 2.96 us  [local(): return total.astype(BF16)]
    unnamed x1 -> x0, local copies, waits for them, and re-layouts: 2.49 us -> none
where the time goes in v3:
time: 71.2 us; the launch traced here: 71 us
  Pallas kernels  68 us (96%)
  other arithmetic  2.96 us (4%)
    pallas_call x1, Pallas kernels, local(): pl.pallas_call(body, out_shape=jax.ShapeDtypeStruct((OUT_ROWS, D), F32),...  68 us
    convert_element_type x1, other arithmetic, local(): return total.astype(BF16)  2.96 us

profile of v3, /device:TPU:1, one launch (start us, length us, event | category | flops | bytes accessed | tf_op | source)
XLA Modules:
  0.0 71.0 jit_solution(12661353873512587423)
XLA Ops:
  0.0 68.0 %shard_map.100 = f32[160,4096]{1,0:T(8,128)} custom-call(bf16[640,4096]{1,0:T(8,128)(2,1)} %tok_hbm.1, bf16[4096,512]{1,0:T(8,128)(2,1)} %wq_hbm.1, bf16[4096,128]{1,0:T(8,128)(2,1)} %wk_hbm.1, bf16[4096,128]{1,0:T(8,128)(2,1)} %wv_hbm.1, bf16[64,4096]{1,0:T(8,128)(2,1)} %bitcast.3, bf16[32,64]{1,0:T(8,128)(2,1)} %pos_ref.1, bf16[8,32]{1,0:T(8,128)(2,1)} %bitcast.4, ...), custom_call_target="tpu_custom_call" | custom-call | tf_op jit(solution)/shard_map/pallas_call | solution.py:658
  68.0 3.0 %convert_element_type.3 = bf16[160,4096]{1,0:T(8,128)(2,1)} convert(f32[160,4096]{1,0:T(8,128)} %shard_map.100) | non-fusion elementwise | flops 655360 | bytes 3932160 | tf_op jit(solution)/shard_map/convert_element_type | solution.py:720

commit v4 on v3

v4 whole, which is shorter than its diff:
```python
import jax
import jax.numpy as jnp
from jax import lax
from jax.experimental import pallas as pl
from jax.experimental.pallas import tpu as pltpu
from jax.sharding import Mesh
from jax.sharding import PartitionSpec as P

HD = 64
CMP = 32
SB = 64
N_SEL = 16
N_KV = 32
N_Z = 4
PLANE = 8
N_TP = 4
ROWS = 640
BLOCKS = 10
GROUPS = 2
GROUP = 4
SPANS = 20
N_SPANS = 640
VMEM_MIB = 58
STRIP = 32
HALVES = (slice(0, 320), slice(320, 640))
WIDTH = 512
OUT_ROWS = 160
D = 4096
CHUNK = 1024
KV = ("kv_0", "kv_1", "kv_2")
KV_TP = ("kv_0", "kv_1", "kv_2", "tp")
MESH = pl.DeviceIdType.MESH
BF16 = jnp.bfloat16
F32 = jnp.float32
LOW = -1e30


def nt_dot(a, b):
    return lax.dot_general(a, b, (((1,), (1,)), ((), ())), preferred_element_type=F32)


def nn_dot(a, b):
    return jnp.dot(a, b, preferred_element_type=F32)


def make_plan(me, chosen_ref, need_ref, index_ref, bias_ref):
    lane = lax.broadcasted_iota(jnp.int32, (BLOCKS, N_SEL), 1)
    spread = lax.broadcasted_iota(jnp.int32, (N_SEL, N_SEL * SB), 1) // SB
    spread = spread == lax.broadcasted_iota(jnp.int32, (N_SEL, N_SEL * SB), 0)
    spread = jnp.where(spread, 1.0, 0.0).astype(BF16)
    need_lane = lax.broadcasted_iota(jnp.int32, (1, 128), 1)
    named = [chosen_ref[:, g, :] for g in range(GROUPS)]
    for g in range(GROUPS):
        repeated = jnp.zeros((BLOCKS, N_SEL), F32)
        for t in range(N_SEL - 1):
            same = jnp.logical_and(named[g] == named[g][:, t : t + 1], lane > t)
            repeated = jnp.where(same, 1.0, repeated)
        bias = nn_dot(repeated.astype(BF16), spread) * LOW
        for b in range(BLOCKS):
            bias_ref[g, b] = bias[b : b + 1]
    places = [n - (n // BLOCKS) * BLOCKS for n in named]
    sources = [n // BLOCKS for n in named]

    def ends(axis_min, value):
        for axis in (0, 1):
            value = axis_min(value, axis=axis, keepdims=True)
        return value

    firsts = [jnp.zeros((BLOCKS, N_SEL), jnp.int32) for _ in range(GROUPS)]
    for s in range(N_KV):
        row = jnp.zeros((1, 128), jnp.int32)
        for g in range(GROUPS):
            hit = sources[g] == s
            first = ends(jnp.min, jnp.where(hit, places[g], BLOCKS - 1))
            last = ends(jnp.max, jnp.where(hit, places[g], 0))
            firsts[g] = jnp.where(hit, first, firsts[g])
            row = jnp.where(need_lane == 2 * g, first, row)
            row = jnp.where(need_lane == 2 * g + 1, last, row)
        need_ref[s // PLANE, s % PLANE] = row
    for g in range(GROUPS):
        away = (sources[g] * GROUPS + g) * 2 + jnp.where(places[g] == firsts[g], 0, 1)
        home = 4 * N_KV + g * BLOCKS + places[g]
        index_ref[g, :BLOCKS, :N_SEL] = jnp.where(sources[g] == me, home, away)


def body(
    tok_hbm,
    wq_hbm,
    wk_hbm,
    wv_hbm,
    wg_hbm,
    pos_ref,
    kmix_ref,
    vmix_ref,
    wo_hbm,
    chosen_ref,
    out_ref,
    tok,
    wq,
    wkv,
    wg,
    acc,
    gates,
    qp,
    sums,
    asked,
    asked_s,
    asked_far,
    asked_far_s,
    table,
    stage,
    unit_0,
    unit_1,
    unit_2,
    comp,
    score,
    prob,
    keys_in,
    values_in,
    span_keys,
    span_values,
    mask,
    need_ref,
    need_s,
    index_ref,
    index_s,
    bias_ref,
    wall,
    att,
    got,
    total_ref,
    load_sem,
    asked_sem,
    w_send,
    w_recv,
    att_send,
    att_recv,
    need_send,
    need_recv,
    far_send,
    far_recv,
    lift_send,
    lift_recv,
    unit_send,
    unit_recv,
    sum_send,
    sum_recv,
    blk_send,
    blk_recv,
):
    kz, ky, kc, x = (lax.axis_index(name) for name in KV_TP)
    kp = ky * 2 + kc
    me = kz * PLANE + kp
    units = (unit_0, unit_1, unit_2)

    def in_plane(p):
        return (kz, p // 2, lax.rem(p, 2), x)

    def above(hops):
        return (lax.rem(kz + hops, N_Z), ky, kc, x)

    left, right, far = (lax.rem(x + hop, N_TP) for hop in (3, 1, 2))
    barrier = pltpu.get_barrier_semaphore()

    def signal(device):
        pl.semaphore_signal(barrier, inc=1, device_id=device, device_id_type=MESH)

    for peer in (left, right, far):
        signal((kz, ky, kc, peer))
    for hops in (1, 2, 3):
        signal(above(hops))
    for hop in range(1, PLANE):
        signal(in_plane(lax.rem(kp + hop, PLANE)))
    edge = jnp.logical_or(kz == 0, kz == N_Z - 1)

    def across(p):
        return (N_Z - 1 - kz, p // 2, lax.rem(p, 2), x)

    @pl.when(edge)
    def _():
        for hop in range(1, PLANE):
            signal(across(lax.rem(kp + hop, PLANE)))

    loads = []

    def load(src, dst):
        loads.append(pltpu.make_async_copy(src, dst, load_sem.at[len(loads)]))
        loads[-1].start()
        return loads[-1]

    steps = D // CHUNK
    kv_loads = []
    for k in range(steps):
        rows = pl.ds(k * CHUNK, CHUNK)
        kv_loads.append(
            (
                load(wk_hbm.at[rows], wkv.at[rows, pl.ds(0, 128)]),
                load(wv_hbm.at[rows], wkv.at[rows, pl.ds(128, 128)]),
                load(tok_hbm.at[:, rows], tok.at[:, rows]),
            )
        )
    wq_load = load(wq_hbm, wq)
    wg_load = load(wg_hbm, wg.at[pl.ds(0, 64)])
    wo_load = load(wo_hbm, wall.at[pl.ds(pl.multiple_of(x * WIDTH, WIDTH), WIDTH)])
    with jax.named_scope("barrier_wait"):
        peers_met = PLANE - 1 + N_Z - 1 + N_TP - 1
        pl.semaphore_wait(barrier, peers_met + jnp.where(edge, PLANE - 1, 0))

    def remote(src, dst, send, recv, device):
        return pltpu.make_async_remote_copy(
            src_ref=src,
            dst_ref=dst,
            send_sem=send,
            recv_sem=recv,
            device_id=device,
            device_id_type=MESH,
        )

    def need_copy(p, sender):
        return remote(
            need_ref.at[:, p], asked.at[sender], need_send.at[p], need_recv.at[sender], in_plane(p)
        )

    def peers(fn):
        def step(p, carry):
            @pl.when(p != kp)
            def _():
                fn(p)

            return carry

        lax.fori_loop(0, PLANE, step, 0)

    color = lax.rem(ky + kz, 2)
    mine_row = color * 256 + kc * 128
    other_row = (1 - color) * 256 + kc * 128

    def region(shard, row, count):
        return wall.at[pl.ds(pl.multiple_of(shard * WIDTH + row, 8), count)]

    def w_copy(index, src, dst, device):
        return remote(src, dst, w_send.at[index], w_recv.at[index], device)

    def w_first(side, piece, receiving=False):
        row = mine_row + 32 * piece
        shard = ((left, right)[side]) if receiving else x
        src = region(shard, row, 32)
        dst = src
        if not receiving:
            src = wo_hbm.at[pl.ds(pl.multiple_of(row, 32), 32)]
        return w_copy(4 * side + piece, src, dst, (kz, ky, kc, (right, left)[side]))

    def w_relay(piece, receiving=False):
        side = piece // 2
        part = region(far if receiving else (left, right)[side], mine_row + 32 * piece, 32)
        return w_copy(8 + piece, part, part, (kz, ky, kc, (right, left)[side]))

    directions = (
        (kz, lax.rem(ky + 1, 4), kc, x),
        (kz, lax.rem(ky + 3, 4), kc, x),
        (lax.rem(kz + 1, 4), ky, kc, x),
        (lax.rem(kz + 3, 4), ky, kc, x),
    )
    shards = (left, right, far)

    def w_second(o, piece, j, receiving=False):
        row = (other_row if receiving else mine_row) + 32 * piece + 8 * j
        part = region(shards[o], row, 8)
        return w_copy(12 + 16 * o + 4 * piece + j, part, part, directions[j])

    def w_third(half, o, piece, receiving=False):
        row = (mine_row, other_row)[half] + 32 * piece
        row = row - kc * 128 + (1 - kc) * 128 if receiving else row
        part = region(shards[o], row, 32)
        return w_copy(60 + 12 * half + 4 * o + piece, part, part, (kz, ky, 1 - kc, x))

    def w_spread(o, piece):
        for j in range(4):
            w_second(o, piece, j).start()
        w_third(0, o, piece).start()

    def w_swap(o):
        for piece in range(4):
            for j in range(4):
                w_second(o, piece, j, True).wait_recv()
            w_third(1, o, piece).start()

    for piece in range(4):
        w_first(0, piece).start()
        w_first(1, (piece + 2) % 4).start()

    with jax.named_scope("plan"):
        make_plan(me, chosen_ref, need_ref, index_ref, bias_ref)
        need_load = pltpu.make_async_copy(need_ref, need_s, load_sem.at[15])
        need_load.start()
        index_load = pltpu.make_async_copy(index_ref, index_s, load_sem.at[16])
        index_load.start()
    peers(lambda p: need_copy(p, kp).start())

    def need_far(p, sender):
        return remote(
            need_ref.at[0, p],
            asked_far.at[sender],
            far_send.at[p],
            far_recv.at[sender],
            across(p),
        )

    def everyone(fn):
        def step(p, carry):
            fn(p)
            return carry

        lax.fori_loop(0, PLANE, step, 0)

    @pl.when(kz == N_Z - 1)
    def _():
        everyone(lambda p: need_far(p, kp).start())

    wg[64:] = jnp.zeros((64, D), BF16)

    def clear(d, carry):
        sums[d // PLANE, lax.rem(d, PLANE)] = jnp.zeros(sums.shape[2:], BF16)
        return carry

    lax.fori_loop(me + 1, N_KV, clear, 0)

    with jax.named_scope("kv_proj"):
        for k in range(steps):
            for copy in kv_loads[k]:
                copy.wait()
            ks = slice(k * CHUNK, (k + 1) * CHUNK)
            for rows in HALVES:
                part = nn_dot(tok[rows, ks], wkv[ks])
                acc[rows, :256] = part if k == 0 else acc[rows, :256] + part
    low = lax.broadcasted_iota(jnp.int32, (ROWS, 128), 1) < HD
    keys = acc[:, :128].astype(BF16).astype(F32)
    values = acc[:, 128:256].astype(BF16).astype(F32)
    pairs = (
        jnp.where(low, keys, pltpu.roll(values, HD, 1)),
        jnp.where(low, pltpu.roll(keys, HD, 1), values),
    )
    offsets = pos_ref[...].astype(F32)
    offsets = jnp.concatenate([offsets, offsets], axis=1)
    lane_low = lax.broadcasted_iota(jnp.int32, (CMP, 128), 1) < HD
    row_head = lax.broadcasted_iota(jnp.int32, (8, CMP), 0)
    diagonal = lax.broadcasted_iota(jnp.int32, (CMP, CMP), 0) == lax.broadcasted_iota(
        jnp.int32, (CMP, CMP), 1
    )

    def column(ref, head):
        row = jnp.sum(jnp.where(row_head == head, ref[...].astype(F32), 0.0), axis=0, keepdims=True)
        return jnp.sum(jnp.where(diagonal, row, 0.0), axis=1, keepdims=True)

    with jax.named_scope("summary"):
        tails = []
        for g in range(GROUPS):
            pair = pairs[g]
            blocks = pair.astype(BF16).reshape(BLOCKS, SB, 128)
            unit_0[g] = blocks
            table[4 * N_KV + g * BLOCKS : 4 * N_KV + (g + 1) * BLOCKS] = blocks
            head = x * GROUPS + g
            mixing = jnp.where(lane_low, column(kmix_ref, head), column(vmix_ref, head))
            spans = jnp.sum((pair.reshape(SPANS, CMP, 128) + offsets[None]) * mixing[None], axis=1)
            sums[kz, kp, 16 * g : 16 * g + 16] = spans[:16].astype(BF16)
            tails.append(spans[16:])
        sums[kz, kp, 32:] = jnp.concatenate(tails, axis=0).astype(BF16)

    def lift_copy(hops, receiving=False):
        part = sums.at[kz - hops if receiving else kz, kp]
        return remote(part, part, lift_send.at[hops], lift_recv.at[hops], above(hops))

    def sum_copy(hops, p, sender):
        part = sums.at[kz - hops, sender]
        k = hops * PLANE
        return remote(part, part, sum_send.at[k + p], sum_recv.at[k + sender], in_plane(p))

    def spread(hops, fn):
        def step(p, carry):
            @pl.when(p > kp if hops == 0 else p != kp)
            def _():
                fn(p)

            return carry

        lax.fori_loop(0, PLANE, step, 0)

    def arriving(hops, fn):
        def step(p, carry):
            @pl.when(p < kp if hops == 0 else p != kp)
            def _():
                fn(p)

            return carry

        lax.fori_loop(0, PLANE, step, 0)

    for hops in (1, 2, 3):

        @pl.when(kz + hops < N_Z)
        def _():
            lift_copy(hops).start()

    spread(0, lambda p: sum_copy(0, p, kp).start())

    def unit_copy(hops):
        return remote(
            units[hops - 1], units[hops], unit_send.at[hops], unit_recv.at[hops], above(1)
        )

    sends_unit = {1: kz < 3, 2: jnp.logical_or(kz == 1, kz == 2)}

    @pl.when(sends_unit[1])
    def _():
        unit_copy(1).start()

    with jax.named_scope("need_wait"):

        def take_need(p):
            need_copy(kp, p).wait_recv()
            pltpu.make_async_copy(asked.at[p], asked_s.at[p], asked_sem.at[p]).start()

        peers(take_need)
        peers(lambda p: pltpu.make_async_copy(asked.at[p], asked_s.at[p], asked_sem.at[p]).wait())
        need_load.wait()
        index_load.wait()

        @pl.when(kz == 0)
        def _():
            def take(p):
                need_far(p, p).wait_recv()
                copy = pltpu.make_async_copy(asked_far.at[p], asked_far_s.at[p], asked_sem.at[p])
                copy.start()
                copy.wait()

            everyone(take)


    def blk_copy(hops, p, sender):
        dst = table.at[pl.ds(((kz - hops) * PLANE + sender) * 4, 4)]
        k = hops * PLANE
        return remote(
            stage.at[hops, p], dst, blk_send.at[k + p], blk_recv.at[k + sender], in_plane(p)
        )

    def serve(hops):
        @pl.when(kz >= hops)
        def _():
            if hops:
                unit_copy(hops).wait_recv()
            if hops == 1:

                @pl.when(sends_unit[2])
                def _():
                    unit_copy(2).start()

            def one(p):
                for slot in range(4):
                    block = asked_s[p, kz - hops, 0, slot]
                    stage[hops, p, slot] = units[hops][slot // 2, block]
                blk_copy(hops, p, kp).start()

            spread(hops, one)
            if hops:
                for slot in range(4):
                    block = need_s[kz - hops, kp, 0, slot]
                    place = ((kz - hops) * PLANE + kp) * 4 + slot
                    table[place] = units[hops][slot // 2, block]

    with jax.named_scope("sum_pass"):
        for hops in (1, 2, 3):

            @pl.when(kz >= hops)
            def _():
                lift_copy(hops, True).wait_recv()
                spread(hops, lambda p: sum_copy(hops, p, kp).start())

    def far_copy(p, sender):
        return remote(
            stage.at[3, p],
            table.at[pl.ds(sender * 4, 4)],
            blk_send.at[3 * PLANE + p],
            blk_recv.at[3 * PLANE + sender],
            across(p),
        )

    with jax.named_scope("serve_0"):
        serve(0)

        @pl.when(kz == 0)
        def _():
            def one(p):
                for slot in range(4):
                    stage[3, p, slot] = unit_0[slot // 2, asked_far_s[p, 0, slot]]
                far_copy(p, kp).start()

            everyone(one)

    with jax.named_scope("q_proj"):
        wq_load.wait()
        for k in range(steps):
            ks = slice(k * CHUNK, (k + 1) * CHUNK)
            part = nn_dot(tok[:, ks], wq[ks])
            acc[...] = part if k == 0 else acc[...] + part
        for h in range(GROUPS * GROUP):
            tile = acc[:, 128 * (h // 2) : 128 * (h // 2) + 128]
            if h % 2:
                tile = pltpu.roll(tile, HD, 1)
            tile = jnp.where(low, tile, 0.0).astype(BF16) * BF16(HD**-0.5)
            qp[:, h // GROUP, h % GROUP] = tile.reshape(BLOCKS, SB, 128)
    with jax.named_scope("gates"):
        wg_load.wait()
        for half, rows in enumerate(HALVES):
            own = pltpu.roll(nt_dot(tok[rows], wg[...]), lax.rem(128 - x * 16, 128), 1)
            part = slice(half * BLOCKS // 2, (half + 1) * BLOCKS // 2)
            gates[part] = jax.nn.sigmoid(own).reshape(BLOCKS // 2, SB, 128)

    with jax.named_scope("sum_wait"):
        for hops in range(N_Z):

            @pl.when(kz >= hops)
            def _():
                arriving(hops, lambda p: sum_copy(hops, kp, p).wait_recv())

    lane = lax.broadcasted_iota(jnp.int32, (SB, N_SPANS), 1)
    tail = lane - N_KV * 16
    span = jnp.where(
        tail < 0,
        (lane // 16) * SPANS + lax.rem(lane, 16),
        (tail // 4) * SPANS + 16 + lax.rem(tail, 4),
    )
    gap = span * CMP + CMP - 1 - lax.broadcasted_iota(jnp.int32, (SB, N_SPANS), 0)
    row_c = lax.rem(lax.broadcasted_iota(jnp.int32, (GROUP * SB, 1), 0), SB)

    def with_ones(pair):
        first = lax.broadcasted_iota(jnp.int32, pair.shape, 1) < HD
        return jnp.where(first, 1.0, pair.astype(F32)).astype(BF16)

    def gate_cols(b, g, branch):
        cols = [
            gates[b][:, 2 * (GROUP * g + r) + branch : 2 * (GROUP * g + r) + branch + 1]
            for r in range(GROUP)
        ]
        return jnp.concatenate(cols, axis=0)

    for g in range(GROUPS):
        tails = [
            sums[s // PLANE, s % PLANE, 32:].astype(F32)[4 * g : 4 * g + 4] for s in range(N_KV)
        ]
        head = sums[:, :, 16 * g : 16 * g + 16].reshape(N_KV * 16, 128)
        tails = jnp.concatenate(tails, axis=0).astype(BF16)
        span_keys[g, : N_KV * 16] = head
        span_keys[g, N_KV * 16 :] = tails
        span_values[g, : N_KV * 16] = with_ones(head)
        span_values[g, N_KV * 16 :] = with_ones(tails)

    def weigh(g, width, biased):
        for c in range(GROUP * SB // STRIP):
            rows = slice(c * STRIP, (c + 1) * STRIP)
            part = biased(score[g, rows, :width], c)
            most = jnp.max(part, axis=1, keepdims=True)
            prob[g, rows, :width] = jnp.exp(part - most).astype(BF16)

    def combine(g, width, table_rows):
        halves = [
            nn_dot(prob[g, h * 128 : (h + 1) * 128, :width], table_rows[...]) for h in range(2)
        ]
        mixed = jnp.concatenate(halves, axis=0)
        return mixed / pltpu.roll(mixed, HD, 1)

    def compressed(b, carry):
        start = me * ROWS + b * SB
        mask[...] = jnp.where(gap <= start, 0.0, LOW)
        for g in range(GROUPS):
            score[g, :, :N_SPANS] = nt_dot(qp[b, g].reshape(GROUP * SB, 128), span_keys[g])

        def biased(part, c):
            first = (c * STRIP) % SB
            return part + mask[first : first + STRIP]

        for g in range(GROUPS):
            weigh(g, N_SPANS, biased)
        for g in range(GROUPS):
            factor = jnp.where(row_c + start >= CMP - 1, gate_cols(b, g, 0), 0.0)
            comp[b, g] = combine(g, N_SPANS, span_values.at[g]) * factor

        @pl.when(b == 0)
        def _():
            with jax.named_scope("serve_1"):
                serve(1)

        @pl.when(b == 1)
        def _():
            with jax.named_scope("relay"):
                for piece in (0, 2, 1, 3):
                    w_first(piece // 2, piece, True).wait_recv()
                    w_relay(piece).start()

        @pl.when(b == BLOCKS - 1)
        def _():
            with jax.named_scope("serve_2"):
                serve(2)

        return carry

    with jax.named_scope("comp"):
        lax.fori_loop(0, BLOCKS, compressed, 0)

    with jax.named_scope("w1_wait"):
        for side in range(2):
            for piece in range(4):
                if piece // 2 != side:
                    w_first(side, piece, True).wait_recv()
                w_spread(side, piece)
    with jax.named_scope("blk_wait"):
        for hops in range(N_Z - 1):

            @pl.when(kz >= hops)
            def _():
                arriving(hops, lambda p: blk_copy(hops, kp, p).wait_recv())

        @pl.when(kz == N_Z - 1)
        def _():
            everyone(lambda p: far_copy(p, p).wait_recv())

    lane_first = lax.broadcasted_iota(jnp.int32, (STRIP, 128), 1)
    row_first = lax.broadcasted_iota(jnp.int32, (STRIP, 128), 0)
    low_half = lax.broadcasted_iota(jnp.int32, (SB, 128), 1) < HD

    def att_copy(target, sender):
        rows = pl.ds(pl.multiple_of(target * OUT_ROWS, 32), OUT_ROWS)
        return remote(
            att.at[rows],
            got.at[sender],
            att_send.at[target],
            att_recv.at[sender],
            (kz, ky, kc, target),
        )

    first_block = lax.rem(5 * (x + 1) // 2, BLOCKS)

    def chosen_block(i, carry):
        b = lax.rem(first_block + i, BLOCKS)
        for g in range(GROUPS):
            for s in range(N_SEL):
                piece = table[index_s[g, b, s]]
                keys_in[g, s * SB : (s + 1) * SB] = piece
                values_in[g, s * SB : (s + 1) * SB] = with_ones(piece)
            score[g] = nt_dot(qp[b, g].reshape(GROUP * SB, 128), keys_in[g])
        for g in range(GROUPS):

            def biased(part, c):
                part = part + bias_ref[g, b]
                seen = lane_first <= row_first + (c * STRIP) % SB
                seen = jnp.logical_or(lane_first >= SB, seen)
                return jnp.concatenate(
                    [jnp.where(seen, part[:, :128], LOW), part[:, 128:]], axis=1
                )

            weigh(g, N_SEL * SB, biased)
        for g in range(GROUPS):
            both = comp[b, g] + combine(g, N_SEL * SB, values_in.at[g]) * gate_cols(b, g, 1)
            for half in range(2):
                even = both[(2 * half) * SB : (2 * half + 1) * SB]
                odd = both[(2 * half + 1) * SB : (2 * half + 2) * SB]
                tile = jnp.where(low_half, pltpu.roll(even, HD, 1), odd).astype(BF16)
                lanes = slice(256 * g + 128 * half, 256 * g + 128 * half + 128)
                att[pl.ds(pl.multiple_of(b * SB, SB), SB), lanes] = tile
        for hop, last in ((1, 2), (2, 5), (3, 7)):

            @pl.when(i == last)
            def _():
                target = lax.rem(x + hop, N_TP)
                att_copy(target, x).start()

        for last, pieces in ((5, (0, 2)), (8, (1, 3))):

            @pl.when(i == last)
            def _():
                with jax.named_scope("w1_far"):
                    for piece in pieces:
                        w_relay(piece, True).wait_recv()
                        w_spread(2, piece)

        return carry

    with jax.named_scope("chosen"):
        lax.fori_loop(0, BLOCKS, chosen_block, 0)

    with jax.named_scope("w2_near"):
        w_swap(0)
        w_swap(1)
    with jax.named_scope("wo_wait"):
        wo_load.wait()
    got[x] = att[pl.ds(pl.multiple_of(x * OUT_ROWS, 32), OUT_ROWS)]
    for order, shard in enumerate((x, left, right, far)):
        if order:
            with jax.named_scope("w3_wait"):
                att_copy(shard, shard).wait_recv()
                for piece in range(4):
                    w_third(0, order - 1, piece, True).wait_recv()
                    w_third(1, order - 1, piece, True).wait_recv()

        def project(n, carry):
            cols = pl.ds(pl.multiple_of(n * CHUNK, CHUNK), CHUNK)
            rows = pl.ds(pl.multiple_of(shard * WIDTH, WIDTH), WIDTH)
            part = nn_dot(got[shard], wall[rows, cols])
            if order:
                part = part + total_ref[:, cols]
            if order < 3:
                total_ref[:, cols] = part
            else:
                out_ref[:, cols] = part.astype(BF16)
            return carry

        with jax.named_scope("outproj"):
            lax.fori_loop(0, D // CHUNK, project, 0)
        if order == 1:
            with jax.named_scope("w2_far"):
                w_swap(2)

    with jax.named_scope("drain"):
        peers(lambda p: need_copy(p, kp).wait_send())

        @pl.when(kz == N_Z - 1)
        def _():
            everyone(lambda p: need_far(p, kp).wait_send())

        @pl.when(kz == 0)
        def _():
            everyone(lambda p: far_copy(p, kp).wait_send())

        for piece in range(4):
            w_first(0, piece).wait_send()
            w_first(1, piece).wait_send()
            w_relay(piece).wait_send()
            for o in range(3):
                for j in range(4):
                    w_second(o, piece, j).wait_send()
                w_third(0, o, piece).wait_send()
                w_third(1, o, piece).wait_send()
        for hop in (1, 2, 3):
            att_copy(lax.rem(x + hop, N_TP), x).wait_send()
        for hops in (1, 2, 3):

            @pl.when(kz + hops < N_Z)
            def _():
                lift_copy(hops).wait_send()

        for hops in (1, 2):

            @pl.when(sends_unit[hops])
            def _():
                unit_copy(hops).wait_send()

        for hops in range(N_Z):

            @pl.when(kz >= hops)
            def _():
                def done(p):
                    sum_copy(hops, p, kp).wait_send()
                    if hops < 3:
                        blk_copy(hops, p, kp).wait_send()

                spread(hops, done)


def local(
    tokens,
    query_weight,
    key_weight,
    value_weight,
    gate_weight,
    summary_pos,
    key_mixing,
    value_mixing,
    out_weight,
    chosen,
):
    any_space = pl.BlockSpec(memory_space=pltpu.HBM)
    vmem = pl.BlockSpec(memory_space=pltpu.VMEM)
    dma = pltpu.SemaphoreType.DMA
    unit = pltpu.VMEM((GROUPS, BLOCKS, SB, 128), BF16)
    requests = (N_Z, PLANE, 1, 128)
    return pl.pallas_call(
        body,
        out_shape=pltpu.VMEM((OUT_ROWS, D), BF16),
        in_specs=[any_space] * 5 + [vmem] * 3 + [any_space, vmem],
        out_specs=vmem,
        scratch_shapes=[
            pltpu.VMEM((ROWS, D), BF16),
            pltpu.VMEM((D, WIDTH), BF16),
            pltpu.VMEM((D, 256), BF16),
            pltpu.VMEM((128, D), BF16),
            pltpu.VMEM((ROWS, WIDTH), F32),
            pltpu.VMEM((BLOCKS, SB, 128), F32),
            pltpu.VMEM((BLOCKS, GROUPS, GROUP, SB, 128), BF16),
            pltpu.VMEM((N_Z, PLANE, 40, 128), BF16),
            pltpu.VMEM((PLANE, N_Z, 1, 128), jnp.int32),
            pltpu.SMEM((PLANE, N_Z, 1, 128), jnp.int32),
            pltpu.VMEM((PLANE, 1, 128), jnp.int32),
            pltpu.SMEM((PLANE, 1, 128), jnp.int32),
            pltpu.VMEM((4 * N_KV + GROUPS * BLOCKS, SB, 128), BF16),
            pltpu.VMEM((N_Z, PLANE, 4, SB, 128), BF16),
            unit,
            unit,
            unit,
            pltpu.VMEM((BLOCKS, GROUPS, GROUP * SB, 128), F32),
            pltpu.VMEM((GROUPS, GROUP * SB, N_SEL * SB), F32),
            pltpu.VMEM((GROUPS, GROUP * SB, N_SEL * SB), BF16),
            pltpu.VMEM((GROUPS, N_SEL * SB, 128), BF16),
            pltpu.VMEM((GROUPS, N_SEL * SB, 128), BF16),
            pltpu.VMEM((GROUPS, N_SPANS, 128), BF16),
            pltpu.VMEM((GROUPS, N_SPANS, 128), BF16),
            pltpu.VMEM((SB, N_SPANS), F32),
            pltpu.VMEM(requests, jnp.int32),
            pltpu.SMEM(requests, jnp.int32),
            pltpu.VMEM((GROUPS, 16, 128), jnp.int32),
            pltpu.SMEM((GROUPS, 16, 128), jnp.int32),
            pltpu.VMEM((GROUPS, BLOCKS, 1, N_SEL * SB), F32),
            pltpu.VMEM((N_TP * WIDTH, D), BF16),
            pltpu.VMEM((ROWS, WIDTH), BF16),
            pltpu.VMEM((N_TP, OUT_ROWS, WIDTH), BF16),
            pltpu.VMEM((OUT_ROWS, D), F32),
            dma((17,)),
            dma((PLANE,)),
            dma((84,)),
            dma((84,)),
            dma((N_TP,)),
            dma((N_TP,)),
            dma((PLANE,)),
            dma((PLANE,)),
            dma((PLANE,)),
            dma((PLANE,)),
            dma((N_Z,)),
            dma((N_Z,)),
            dma((N_Z,)),
            dma((N_Z,)),
            dma((N_KV,)),
            dma((N_KV,)),
            dma((N_KV,)),
            dma((N_KV,)),
        ],
        compiler_params=pltpu.CompilerParams(
            collective_id=0, has_side_effects=True, vmem_limit_bytes=VMEM_MIB * 1024 * 1024
        ),
    )(
        tokens,
        query_weight,
        key_weight,
        value_weight,
        gate_weight.T,
        summary_pos,
        key_mixing.T,
        value_mixing.T,
        out_weight,
        chosen,
    )


def solution(mesh):
    torus = Mesh(mesh.devices.reshape(4, 4, 2, mesh.shape["tp"]), ("kv_0", "kv_1", "kv_2", "tp"))
    in_specs = (
        P(KV, None),
        P(None, "tp"),
        P(None, "tp"),
        P(None, "tp"),
        P(),
        P(),
        P(),
        P(),
        P("tp", None),
        P(KV, "tp", None),
    )
    out_specs = P(KV_TP, None)
    return jax.shard_map(local, mesh=torus, in_specs=in_specs, out_specs=out_specs, check_vma=False)
```

time: 71.2 us -> 61.8 us (0.87)
  Pallas kernels: 68 us -> 60.6 us
  other arithmetic: 2.96 us -> 0 us
  local copies, waits for them, and re-layouts: 0 us -> 1.06 us
    pallas_call x1, Pallas kernels: 68 us -> 60.6 us  [local(): pl.pallas_call(body, out_shape=pltpu.VMEM((OUT_ROWS, D), BF16), in_specs=...]
    convert_element_type x1 -> x0, other arithmetic: 2.96 us -> none  [local(): return total.astype(BF16)]
    unnamed x0 -> x1, local copies, waits for them, and re-layouts: none -> 1.06 us
where the time goes in v4:
time: 61.8 us; the launch traced here: 61.7 us
  Pallas kernels  60.6 us (98%)
  local copies, waits for them, and re-layouts  1.06 us (2%)
    pallas_call x1, Pallas kernels, local(): pl.pallas_call(body, out_shape=pltpu.VMEM((OUT_ROWS, D), BF16), in_specs=...  60.6 us

profile of v4, /device:TPU:1, one launch (start us, length us, event | category | flops | bytes accessed | tf_op | source)
XLA Modules:
  0.0 61.7 jit_solution(11240458426055089674)
XLA Ops:
  0.0 60.6 %shard_map.100 = bf16[160,4096]{1,0:T(8,128)(2,1)S(1)} custom-call(bf16[640,4096]{1,0:T(8,128)(2,1)} %tok_hbm.1, bf16[4096,512]{1,0:T(8,128)(2,1)} %wq_hbm.1, bf16[4096,128]{1,0:T(8,128)(2,1)} %wk_hbm.1, bf16[4096,128]{1,0:T(8,128)(2,1)} %wv_hbm.1, bf16[64,4096]{1,0:T(8,128)(2,1)} %bitcast.3, bf16[32,64]{1,0:T(8,128)(2,1)} %pos_ref.1, ...), custom_call_target="tpu_custom_call" | custom-call | tf_op jit(solution)/shard_map/pallas_call | solution.py:785
  60.6 1.1 %copy.12 = bf16[160,4096]{1,0:T(8,128)(2,1)} copy(bf16[160,4096]{1,0:T(8,128)(2,1)S(1)} %shard_map.100) | data formatting | bytes 2621440

commit v5 on v4

--- a/solution.py
+++ b/solution.py
@@ -18,6 +18,7 @@
 BLOCKS = 10
 GROUPS = 2
 GROUP = 4
+DIRECTIONS = ((0, 0, 8), (1, 8, 8), (2, 16, 8), (3, 24, 8))
 SPANS = 20
 N_SPANS = 640
 VMEM_MIB = 58
@@ -43,13 +44,36 @@
     return jnp.dot(a, b, preferred_element_type=F32)
 
 
-def make_plan(me, chosen_ref, need_ref, index_ref, bias_ref):
+def plan_requests(chosen_ref, need_ref):
+    need_lane = lax.broadcasted_iota(jnp.int32, (1, 128), 1)
+    named = [chosen_ref[:, g, :] for g in range(GROUPS)]
+    sources = [n // BLOCKS for n in named]
+    places = [n - s * BLOCKS for n, s in zip(named, sources)]
+    firsts = [jnp.zeros((BLOCKS, N_SEL), jnp.int32) for _ in range(GROUPS)]
+    for s in range(N_KV):
+        ends = []
+        for g in range(GROUPS):
+            hit = sources[g] == s
+            low = jnp.where(hit, BLOCKS - 1 - places[g], 0)
+            high = jnp.where(hit, places[g], 0)
+            ends += [jnp.max(v, axis=0, keepdims=True) for v in (low, high)]
+        ends = jnp.max(jnp.concatenate(ends, axis=0), axis=1, keepdims=True)
+        row = jnp.zeros((1, 128), jnp.int32)
+        for g in range(GROUPS):
+            first = BLOCKS - 1 - ends[2 * g : 2 * g + 1]
+            firsts[g] = jnp.where(sources[g] == s, first, firsts[g])
+            row = jnp.where(need_lane == 2 * g, first, row)
+            row = jnp.where(need_lane == 2 * g + 1, ends[2 * g + 1 : 2 * g + 2], row)
+        need_ref[s // PLANE, s % PLANE] = row
+    return named, sources, places, firsts
+
+
+def plan_blocks(me, plan, index_ref, bias_ref):
+    named, sources, places, firsts = plan
     lane = lax.broadcasted_iota(jnp.int32, (BLOCKS, N_SEL), 1)
     spread = lax.broadcasted_iota(jnp.int32, (N_SEL, N_SEL * SB), 1) // SB
     spread = spread == lax.broadcasted_iota(jnp.int32, (N_SEL, N_SEL * SB), 0)
     spread = jnp.where(spread, 1.0, 0.0).astype(BF16)
-    need_lane = lax.broadcasted_iota(jnp.int32, (1, 128), 1)
-    named = [chosen_ref[:, g, :] for g in range(GROUPS)]
     for g in range(GROUPS):
         repeated = jnp.zeros((BLOCKS, N_SEL), F32)
         for t in range(N_SEL - 1):
@@ -58,26 +82,6 @@
         bias = nn_dot(repeated.astype(BF16), spread) * LOW
         for b in range(BLOCKS):
             bias_ref[g, b] = bias[b : b + 1]
-    places = [n - (n // BLOCKS) * BLOCKS for n in named]
-    sources = [n // BLOCKS for n in named]
-
-    def ends(axis_min, value):
-        for axis in (0, 1):
-            value = axis_min(value, axis=axis, keepdims=True)
-        return value
-
-    firsts = [jnp.zeros((BLOCKS, N_SEL), jnp.int32) for _ in range(GROUPS)]
-    for s in range(N_KV):
-        row = jnp.zeros((1, 128), jnp.int32)
-        for g in range(GROUPS):
-            hit = sources[g] == s
-            first = ends(jnp.min, jnp.where(hit, places[g], BLOCKS - 1))
-            last = ends(jnp.max, jnp.where(hit, places[g], 0))
-            firsts[g] = jnp.where(hit, first, firsts[g])
-            row = jnp.where(need_lane == 2 * g, first, row)
-            row = jnp.where(need_lane == 2 * g + 1, last, row)
-        need_ref[s // PLANE, s % PLANE] = row
-    for g in range(GROUPS):
         away = (sources[g] * GROUPS + g) * 2 + jnp.where(places[g] == firsts[g], 0, 1)
         home = 4 * N_KV + g * BLOCKS + places[g]
         index_ref[g, :BLOCKS, :N_SEL] = jnp.where(sources[g] == me, home, away)
@@ -263,10 +267,26 @@
     )
     shards = (left, right, far)
 
-    def w_second(o, piece, j, receiving=False):
-        row = (other_row if receiving else mine_row) + 32 * piece + 8 * j
-        part = region(shards[o], row, 8)
-        return w_copy(12 + 16 * o + 4 * piece + j, part, part, directions[j])
+    def slices(o, piece):
+        return ((2, 0, 16), (3, 24, 8)) if piece // 2 == o else DIRECTIONS
+
+    def w_second(o, piece, j, first, count, receiving=False, way=None):
+        row = (other_row if receiving else mine_row) + 32 * piece + first
+        part = region(shards[o], row, count)
+        device = directions[j if way is None else way]
+        return w_copy(12 + 16 * o + 4 * piece + j, part, part, device)
+
+    def w_swing(o, piece, fn, receiving=False):
+        if piece // 2 == o:
+            last = kz == N_Z - 1
+
+            @pl.when(jnp.logical_not(last) if receiving else kz != 0)
+            def _():
+                fn(w_second(o, piece, 1, 16, 8, receiving, 3))
+
+            @pl.when(last if receiving else kz == N_Z - 2)
+            def _():
+                fn(w_second(o, piece, 0, 16, 8, receiving, 2))
 
     def w_third(half, o, piece, receiving=False):
         row = (mine_row, other_row)[half] + 32 * piece
@@ -275,14 +295,16 @@
         return w_copy(60 + 12 * half + 4 * o + piece, part, part, (kz, ky, 1 - kc, x))
 
     def w_spread(o, piece):
-        for j in range(4):
-            w_second(o, piece, j).start()
+        for cut in slices(o, piece):
+            w_second(o, piece, *cut).start()
+        w_swing(o, piece, lambda copy: copy.start())
         w_third(0, o, piece).start()
 
-    def w_swap(o):
-        for piece in range(4):
-            for j in range(4):
-                w_second(o, piece, j, True).wait_recv()
+    def w_swap(o, pieces):
+        for piece in pieces:
+            for cut in slices(o, piece):
+                w_second(o, piece, *cut, True).wait_recv()
+            w_swing(o, piece, lambda copy: copy.wait_recv(), True)
             w_third(1, o, piece).start()
 
     for piece in range(4):
@@ -290,11 +312,9 @@
         w_first(1, (piece + 2) % 4).start()
 
     with jax.named_scope("plan"):
-        make_plan(me, chosen_ref, need_ref, index_ref, bias_ref)
+        plan = plan_requests(chosen_ref, need_ref)
         need_load = pltpu.make_async_copy(need_ref, need_s, load_sem.at[15])
         need_load.start()
-        index_load = pltpu.make_async_copy(index_ref, index_s, load_sem.at[16])
-        index_load.start()
     peers(lambda p: need_copy(p, kp).start())
 
     def need_far(p, sender):
@@ -403,17 +423,28 @@
 
     spread(0, lambda p: sum_copy(0, p, kp).start())
 
-    def unit_copy(hops):
-        return remote(
-            units[hops - 1], units[hops], unit_send.at[hops], unit_recv.at[hops], above(1)
-        )
+    def unit_copy(hops, g):
+        src, dst, k = units[hops - 1].at[g], units[hops].at[g], hops * GROUPS + g
+        return remote(src, dst, unit_send.at[k], unit_recv.at[k], above(1))
 
     sends_unit = {1: kz < 3, 2: jnp.logical_or(kz == 1, kz == 2)}
 
     @pl.when(sends_unit[1])
     def _():
-        unit_copy(1).start()
-
+        for g in range(GROUPS):
+            unit_copy(1, g).start()
+
+    with jax.named_scope("gates"):
+        wg_load.wait()
+        for half, rows in enumerate(HALVES):
+            own = pltpu.roll(nt_dot(tok[rows], wg[...]), lax.rem(128 - x * 16, 128), 1)
+            part = slice(half * BLOCKS // 2, (half + 1) * BLOCKS // 2)
+            gates[part] = jax.nn.sigmoid(own).reshape(BLOCKS // 2, SB, 128)
+
+    with jax.named_scope("plan_blocks"):
+        plan_blocks(me, plan, index_ref, bias_ref)
+        index_load = pltpu.make_async_copy(index_ref, index_s, load_sem.at[16])
+        index_load.start()
     with jax.named_scope("need_wait"):
 
         def take_need(p):
@@ -443,16 +474,21 @@
             stage.at[hops, p], dst, blk_send.at[k + p], blk_recv.at[k + sender], in_plane(p)
         )
 
+    def unit_pass(g):
+        unit_copy(1, g).wait_recv()
+
+        @pl.when(sends_unit[2])
+        def _():
+            unit_copy(2, g).start()
+
     def serve(hops):
         @pl.when(kz >= hops)
         def _():
-            if hops:
-                unit_copy(hops).wait_recv()
             if hops == 1:
-
-                @pl.when(sends_unit[2])
-                def _():
-                    unit_copy(2).start()
+                unit_pass(1)
+            if hops == 2:
+                for g in range(GROUPS):
+                    unit_copy(2, g).wait_recv()
 
             def one(p):
                 for slot in range(4):
@@ -508,12 +544,14 @@
                 tile = pltpu.roll(tile, HD, 1)
             tile = jnp.where(low, tile, 0.0).astype(BF16) * BF16(HD**-0.5)
             qp[:, h // GROUP, h % GROUP] = tile.reshape(BLOCKS, SB, 128)
-    with jax.named_scope("gates"):
-        wg_load.wait()
-        for half, rows in enumerate(HALVES):
-            own = pltpu.roll(nt_dot(tok[rows], wg[...]), lax.rem(128 - x * 16, 128), 1)
-            part = slice(half * BLOCKS // 2, (half + 1) * BLOCKS // 2)
-            gates[part] = jax.nn.sigmoid(own).reshape(BLOCKS // 2, SB, 128)
+    with jax.named_scope("relay"):
+        for piece in (0, 2):
+            w_first(piece // 2, piece, True).wait_recv()
+            w_relay(piece).start()
+
+        @pl.when(kz >= 1)
+        def _():
+            unit_pass(0)
 
     with jax.named_scope("sum_wait"):
         for hops in range(N_Z):
@@ -592,11 +630,17 @@
         @pl.when(b == 1)
         def _():
             with jax.named_scope("relay"):
-                for piece in (0, 2, 1, 3):
+                for piece in (1, 3):
                     w_first(piece // 2, piece, True).wait_recv()
                     w_relay(piece).start()
 
-        @pl.when(b == BLOCKS - 1)
+        @pl.when(b == 4)
+        def _():
+            for side in range(2):
+                for piece in (2 * side, 2 * side + 1):
+                    w_spread(side, piece)
+
+        @pl.when(b == 6)
         def _():
             with jax.named_scope("serve_2"):
                 serve(2)
@@ -606,12 +650,6 @@
     with jax.named_scope("comp"):
         lax.fori_loop(0, BLOCKS, compressed, 0)
 
-    with jax.named_scope("w1_wait"):
-        for side in range(2):
-            for piece in range(4):
-                if piece // 2 != side:
-                    w_first(side, piece, True).wait_recv()
-                w_spread(side, piece)
     with jax.named_scope("blk_wait"):
         for hops in range(N_Z - 1):
 
@@ -638,6 +676,11 @@
         )
 
     first_block = lax.rem(5 * (x + 1) // 2, BLOCKS)
+
+    def pass_far(pieces):
+        for piece in pieces:
+            w_relay(piece, True).wait_recv()
+            w_spread(2, piece)
 
     def chosen_block(i, carry):
         b = lax.rem(first_block + i, BLOCKS)
@@ -673,23 +716,44 @@
                 target = lax.rem(x + hop, N_TP)
                 att_copy(target, x).start()
 
-        for last, pieces in ((5, (0, 2)), (8, (1, 3))):
-
-            @pl.when(i == last)
-            def _():
-                with jax.named_scope("w1_far"):
-                    for piece in pieces:
-                        w_relay(piece, True).wait_recv()
-                        w_spread(2, piece)
+        @pl.when(i == 1)
+        def _():
+            with jax.named_scope("w1_near"):
+                for side in range(2):
+                    for piece in (2 - 2 * side, 3 - 2 * side):
+                        w_first(side, piece, True).wait_recv()
+                        w_spread(side, piece)
+
+        @pl.when(i == BLOCKS - 1)
+        def _():
+            with jax.named_scope("w2_early"):
+                for side in range(2):
+                    w_swap(side, (2 * side, 2 * side + 1))
+
+        @pl.when(i == jnp.where(kz == 0, 5, 4))
+        def _():
+            with jax.named_scope("w1_far"):
+                pass_far((0, 2))
+
+        @pl.when(jnp.logical_and(i == 7, kz != 0))
+        def _():
+            with jax.named_scope("w1_far"):
+                pass_far((1, 3))
 
         return carry
 
     with jax.named_scope("chosen"):
         lax.fori_loop(0, BLOCKS, chosen_block, 0)
 
+    @pl.when(kz == 0)
+    def _():
+        with jax.named_scope("w1_far"):
+            pass_far((1, 3))
+
+
     with jax.named_scope("w2_near"):
-        w_swap(0)
-        w_swap(1)
+        w_swap(0, (2, 3))
+        w_swap(1, (0, 1))
     with jax.named_scope("wo_wait"):
         wo_load.wait()
     got[x] = att[pl.ds(pl.multiple_of(x * OUT_ROWS, 32), OUT_ROWS)]
@@ -717,7 +781,7 @@
             lax.fori_loop(0, D // CHUNK, project, 0)
         if order == 1:
             with jax.named_scope("w2_far"):
-                w_swap(2)
+                w_swap(2, range(4))
 
     with jax.named_scope("drain"):
         peers(lambda p: need_copy(p, kp).wait_send())
@@ -735,8 +799,9 @@
             w_first(1, piece).wait_send()
             w_relay(piece).wait_send()
             for o in range(3):
-                for j in range(4):
-                    w_second(o, piece, j).wait_send()
+                for cut in slices(o, piece):
+                    w_second(o, piece, *cut).wait_send()
+                w_swing(o, piece, lambda copy: copy.wait_send())
                 w_third(0, o, piece).wait_send()
                 w_third(1, o, piece).wait_send()
         for hop in (1, 2, 3):
@@ -751,7 +816,8 @@
 
             @pl.when(sends_unit[hops])
             def _():
-                unit_copy(hops).wait_send()
+                for g in range(GROUPS):
+                    unit_copy(hops, g).wait_send()
 
         for hops in range(N_Z):
 
@@ -834,8 +900,8 @@
             dma((PLANE,)),
             dma((N_Z,)),
             dma((N_Z,)),
-            dma((N_Z,)),
-            dma((N_Z,)),
+            dma((N_Z * GROUPS,)),
+            dma((N_Z * GROUPS,)),
             dma((N_KV,)),
             dma((N_KV,)),
             dma((N_KV,)),

time: 61.8 us -> 60.3 us (0.976)
  Pallas kernels: 60.6 us -> 59.1 us
    pallas_call x1, Pallas kernels: 60.6 us -> 59.1 us  [local(): pl.pallas_call(body, out_shape=pltpu.VMEM((OUT_ROWS, D), BF16), in_specs=...]
where the time goes in v5:
time: 60.3 us; the launch traced here: 60.2 us
  Pallas kernels  59.1 us (98%)
  local copies, waits for them, and re-layouts  1.06 us (2%)
    pallas_call x1, Pallas kernels, local(): pl.pallas_call(body, out_shape=pltpu.VMEM((OUT_ROWS, D), BF16), in_specs=...  59.1 us

profile of v5, /device:TPU:1, one launch (start us, length us, event | category | flops | bytes accessed | tf_op | source)
XLA Modules:
  0.0 60.2 jit_solution(4626188731652733978)
XLA Ops:
  0.0 59.1 %shard_map.100 = bf16[160,4096]{1,0:T(8,128)(2,1)S(1)} custom-call(bf16[640,4096]{1,0:T(8,128)(2,1)} %tok_hbm.1, bf16[4096,512]{1,0:T(8,128)(2,1)} %wq_hbm.1, bf16[4096,128]{1,0:T(8,128)(2,1)} %wk_hbm.1, bf16[4096,128]{1,0:T(8,128)(2,1)} %wv_hbm.1, bf16[64,4096]{1,0:T(8,128)(2,1)} %bitcast.3, bf16[32,64]{1,0:T(8,128)(2,1)} %pos_ref.1, ...), custom_call_target="tpu_custom_call" | custom-call | tf_op jit(solution)/shard_map/pallas_call | solution.py:851
  59.1 1.1 %copy.12 = bf16[160,4096]{1,0:T(8,128)(2,1)} copy(bf16[160,4096]{1,0:T(8,128)(2,1)S(1)} %shard_map.100) | data formatting | bytes 2621440

commit v6 on v5

--- a/solution.py
+++ b/solution.py
@@ -716,7 +716,7 @@
                 target = lax.rem(x + hop, N_TP)
                 att_copy(target, x).start()
 
-        @pl.when(i == 1)
+        @pl.when(i == jnp.where(kz == 0, 1, 0))
         def _():
             with jax.named_scope("w1_near"):
                 for side in range(2):
@@ -730,7 +730,7 @@
                 for side in range(2):
                     w_swap(side, (2 * side, 2 * side + 1))
 
-        @pl.when(i == jnp.where(kz == 0, 5, 4))
+        @pl.when(i == jnp.where(kz == 0, 5, 3))
         def _():
             with jax.named_scope("w1_far"):
                 pass_far((0, 2))

time: 60.3 us -> 60.3 us (level)
  no operation moved by 1% of the time
where the time goes in v6:
time: 60.3 us; the launch traced here: 60.2 us
  Pallas kernels  59.1 us (98%)
  local copies, waits for them, and re-layouts  1.06 us (2%)
    pallas_call x1, Pallas kernels, local(): pl.pallas_call(body, out_shape=pltpu.VMEM((OUT_ROWS, D), BF16), in_specs=...  59.1 us

profile of v6, /device:TPU:1, one launch (start us, length us, event | category | flops | bytes accessed | tf_op | source)
XLA Modules:
  0.0 60.2 jit_solution(11299702453727805694)
XLA Ops:
  0.0 59.1 %shard_map.100 = bf16[160,4096]{1,0:T(8,128)(2,1)S(1)} custom-call(bf16[640,4096]{1,0:T(8,128)(2,1)} %tok_hbm.1, bf16[4096,512]{1,0:T(8,128)(2,1)} %wq_hbm.1, bf16[4096,128]{1,0:T(8,128)(2,1)} %wk_hbm.1, bf16[4096,128]{1,0:T(8,128)(2,1)} %wv_hbm.1, bf16[64,4096]{1,0:T(8,128)(2,1)} %bitcast.3, bf16[32,64]{1,0:T(8,128)(2,1)} %pos_ref.1, ...), custom_call_target="tpu_custom_call" | custom-call | tf_op jit(solution)/shard_map/pallas_call | solution.py:851
  59.1 1.1 %copy.12 = bf16[160,4096]{1,0:T(8,128)(2,1)} copy(bf16[160,4096]{1,0:T(8,128)(2,1)S(1)} %shard_map.100) | data formatting | bytes 2621440
